TPU v7x, 128 devices: a whole 4x4x4 slice. The times are simulated.
128 devices in a mesh: sp: 64 (over z, y, x), tp: 2 (over core).
Axes of the slice: x: 4, y: 4, z: 4, core: 2. Of those that a mesh axis runs over, the one named last changes fastest.
Arguments:
- conv_out: bfloat16 [8192, 2048], P('sp', 'tp'), may hold values from -1500 to 1500
- ln_gain: float32 [2048], P('tp'), may hold values from 0.1 to 1.9
- taps: bfloat16 [31, 2048], P(None, 'tp'), may hold values from -1 to 1
- proj_weight: bfloat16 [2048, 2048], P('sp', 'tp'), may hold values from -0.125 to 0.125
- stream_mid: bfloat16 [8192, 2048], P('sp', 'tp'), may hold values from -6 to 6
- out_grad: bfloat16 [8192, 2048], P('sp', 'tp'), may hold values from -16 to 16
- routes: int32 [8192, 2], P('sp'), may hold values from 0 to 31, all different within a row; in each aligned block of 128 rows (0 to 127, 128 to 255, ...) at most 12 rows name the same one
- route_probs: float32 [8192, 2], P('sp'), may hold values from 0.2 to 1
- gate_slabs: bfloat16 [64, 2048, 1792], P('sp', None, 'tp'), may hold values from -0.125 to 0.125
- up_slabs: bfloat16 [64, 2048, 1792], P('sp', None, 'tp'), may hold values from -0.125 to 0.125
- down_slabs: bfloat16 [64, 1792, 2048], P('sp', 'tp'), may hold values from -0.09375 to 0.09375
Outputs:
- grad_input: bfloat16 [8192, 2048], P('sp', 'tp')
- grad_proj: float32 [2048, 2048], P('sp', 'tp')
- grad_gate: bfloat16 [64, 2048, 1792], P('sp', None, 'tp')
- grad_up: bfloat16 [64, 2048, 1792], P('sp', None, 'tp')
- grad_down: bfloat16 [64, 1792, 2048], P('sp', 'tp')
Inputs may be any that keep to these rules, and one draw needn't show every extreme that they name: `routes`: each row names two different experts. Among the rows of one device no expert is named more than 12 times, and in every draw some device's rows name some expert exactly 12 times.
All inputs are finite; a program needn't handle non-finite values.
Results may differ from a plain program's by a relative error of at most 0.015.
Values may be sent and summed in bfloat16 or wider, within the bound.
A program may use at most 128 MiB of HBM per device.

v0:
```python
import jax
import jax.numpy as jnp
from jax import lax
from jax.sharding import PartitionSpec as P

D = 2048


def in_one_piece(arrays, axis, dim, along):
    widths = [a.shape[along] for a in arrays]
    both = jnp.concatenate(arrays, axis=along)
    out = lax.all_gather(both, axis, axis=dim, tiled=True)
    return tuple(jnp.split(out, [sum(widths[:k]) for k in range(1, len(widths))], axis=along))


def cut_along(array, dim, peers):
    before, after = (array.shape[:dim], array.shape[dim + 1 :])
    return jnp.moveaxis(array.reshape(*before, peers, -1, *after), dim, 0)


def summed_on_arrival(array, axis, dim):
    blocks = cut_along(array, dim, lax.axis_size(axis))
    arrived = lax.all_to_all(blocks, axis, split_axis=0, concat_axis=0, tiled=True)
    return arrived.astype(jnp.float32).sum(axis=0)


def total_of_pieces(array, axis):
    return lax.all_gather(array, axis).sum(0)


def copy_for_each(array, axis):
    peers = lax.axis_size(axis)
    return lax.all_to_all(
        jnp.broadcast_to(array[None], (peers, *array.shape)), axis, 0, 0, tiled=True
    )


def joined_along(blocks, dim):
    shape = list(blocks.shape[1:])
    shape[dim] *= blocks.shape[0]
    return jnp.moveaxis(blocks, 0, dim).reshape(shape)


def gather_directly(array, axis, dim):
    blocks = copy_for_each(array, axis)
    return joined_along(blocks, dim)


def passed_along(value, axis, steps):
    count = lax.axis_size(axis)
    first, last = (max(0, -steps), min(count, count - steps))
    return lax.ppermute(value, axis, [(source, source + steps) for source in range(first, last)])


def dispatch_table(route_block, experts, capacity):
    tok_rows = route_block.shape[0]
    labels = jnp.arange(experts, dtype=jnp.int32)
    onehot = (route_block[:, :, None] == labels[None, None, :]).astype(jnp.float32)
    per_token = jnp.sum(onehot, axis=1)
    earlier = (jnp.arange(tok_rows)[:, None] > jnp.arange(tok_rows)[None, :]).astype(jnp.float32)
    before = jnp.dot(earlier, per_token)
    slot_index = jnp.sum(onehot * before[:, None, :], axis=2).astype(jnp.int32)
    position = route_block * capacity + slot_index
    columns = jnp.arange(experts * capacity, dtype=jnp.int32)
    first_pick = position[:, 0:1] == columns[None, :]
    second_pick = position[:, 1:2] == columns[None, :]
    return (first_pick, second_pick)


def contract_rows(left, right):
    return lax.dot_general(
        left, right, (((0,), (0,)), ((), ())), preferred_element_type=jnp.float32
    )


def contract_cols(left, right):
    return lax.dot_general(
        left, right, (((1,), (1,)), ((), ())), preferred_element_type=jnp.float32
    )


def on_device(
    conv_out,
    ln_gain,
    taps,
    proj_weight,
    stream_mid,
    out_grad,
    routes,
    route_probs,
    gate_slabs,
    up_slabs,
    down_slabs,
):
    tok_rows = conv_out.shape[0]
    experts = lax.axis_size("sp") // 2
    capacity = 3 * tok_rows // experts
    first_pick, second_pick = dispatch_table(routes, experts, capacity)
    route_table = (first_pick | second_pick).astype(jnp.bfloat16)
    slot_probs = jnp.sum(
        first_pick.astype(jnp.float32) * route_probs[:, 0:1]
        + second_pick.astype(jnp.float32) * route_probs[:, 1:2],
        axis=0,
    )
    probs_out = jnp.repeat(slot_probs.reshape(experts, capacity), 2, axis=0)

    def packed(source):
        filled = contract_rows(route_table, source).astype(jnp.bfloat16)
        return jnp.repeat(filled.reshape(experts, capacity, source.shape[1]), 2, axis=0)

    half_mid, half_grad, arrived_probs = (
        lax.all_to_all(packed(stream_mid), "sp", split_axis=0, concat_axis=0, tiled=True),
        lax.all_to_all(packed(out_grad), "sp", split_axis=0, concat_axis=0, tiled=True),
        lax.all_to_all(
            probs_out.astype(jnp.bfloat16), "sp", split_axis=0, concat_axis=0, tiled=True
        ).astype(probs_out.dtype),
    )
    arrived_mid, arrived_grad = in_one_piece((half_mid, half_grad), "tp", 2, 0)
    slot_rows = arrived_mid.shape[0] * arrived_mid.shape[1]
    expert_in = arrived_mid.reshape(slot_rows, arrived_mid.shape[2])
    expert_grad = arrived_grad.reshape(slot_rows, arrived_grad.shape[2])
    weight = arrived_probs.reshape(slot_rows, 1)
    w_gate = gate_slabs[0]
    w_up = up_slabs[0]
    w_down = down_slabs[0]
    gate_value = jnp.dot(expert_in, w_gate, preferred_element_type=jnp.float32)
    up_value = jnp.dot(expert_in, w_up, preferred_element_type=jnp.float32)
    gate_sig = jax.nn.sigmoid(gate_value)
    hidden_act = gate_value * gate_sig * up_value
    scaled = (weight * hidden_act).astype(jnp.bfloat16)
    grad_down = contract_rows(scaled, expert_grad).astype(jnp.bfloat16)
    grad_hidden = weight * contract_cols(expert_grad, w_down)
    grad_gate_pre = (
        grad_hidden * up_value * gate_sig * (1.0 + gate_value * (1.0 - gate_sig))
    ).astype(jnp.bfloat16)
    grad_up_pre = (grad_hidden * gate_value * gate_sig).astype(jnp.bfloat16)
    grad_gate = contract_rows(expert_in, grad_gate_pre).astype(jnp.bfloat16)
    grad_up = contract_rows(expert_in, grad_up_pre).astype(jnp.bfloat16)
    partial_value = contract_cols(grad_gate_pre, w_gate) + contract_cols(grad_up_pre, w_up)
    summed = summed_on_arrival(partial_value.astype(jnp.bfloat16), "tp", 1).astype(jnp.bfloat16)
    returned = lax.all_to_all(
        summed.reshape(arrived_mid.shape[0], capacity, summed.shape[1]),
        "sp",
        split_axis=0,
        concat_axis=0,
        tiled=True,
    )
    pair_rows = returned.reshape(experts, 2, capacity, returned.shape[2])
    contrib = jnp.dot(
        route_table,
        pair_rows[:, 0].reshape(experts * capacity, returned.shape[2]),
        preferred_element_type=jnp.float32,
    )
    contrib = contrib + jnp.dot(
        route_table,
        pair_rows[:, 1].reshape(experts * capacity, returned.shape[2]),
        preferred_element_type=jnp.float32,
    )
    grad_stream = (out_grad.astype(jnp.float32) + contrib).astype(jnp.bfloat16)
    values = conv_out.astype(jnp.float32)
    row_total, row_squares = (
        total_of_pieces(jnp.sum(values, axis=1), "tp"),
        total_of_pieces(jnp.sum(values * values, axis=1), "tp"),
    )
    row_mean = row_total[:, None] / D
    row_var = row_squares[:, None] / D - row_mean * row_mean
    inv_std = lax.rsqrt(row_var + 1e-06)
    normed = (values - row_mean) * inv_std
    scaled_z = normed * ln_gain[None, :]
    z_sig = jax.nn.sigmoid(scaled_z)
    activated = (scaled_z * z_sig).astype(jnp.bfloat16)
    whole_stream = gather_directly(grad_stream, "tp", 1)
    selected = whole_stream
    grad_act = jnp.dot(
        selected,
        lax.all_gather(proj_weight, "sp", axis=0, tiled=True),
        preferred_element_type=jnp.float32,
    )
    grad_normed = grad_act * z_sig * (1.0 + scaled_z * (1.0 - z_sig)) * ln_gain[None, :]
    first_sum, second_sum = (
        total_of_pieces(jnp.sum(grad_normed, axis=1), "tp"),
        total_of_pieces(jnp.sum(grad_normed * normed, axis=1), "tp"),
    )
    grad_conv = (
        inv_std * (grad_normed - first_sum[:, None] / D - normed * second_sum[:, None] / D)
    ).astype(jnp.bfloat16)
    reach_rows = taps.shape[0] - 1
    following = passed_along(grad_conv[:reach_rows], "sp", -1)
    extended = jnp.concatenate([grad_conv, following], axis=0).astype(jnp.float32)
    tap_values = taps.astype(jnp.float32)
    grad_input = jnp.zeros((tok_rows, grad_conv.shape[1]), jnp.float32)
    for offset in range(taps.shape[0]):
        grad_input = grad_input + tap_values[offset][None, :] * extended[offset : offset + tok_rows]
    selected = whole_stream
    grad_proj = summed_on_arrival(contract_rows(selected, activated).astype(jnp.bfloat16), "sp", 0)
    return (
        grad_input.astype(jnp.bfloat16),
        grad_proj,
        grad_gate[None],
        grad_up[None],
        grad_down[None],
    )


def solution(mesh):
    return jax.shard_map(
        on_device,
        mesh=mesh,
        in_specs=(
            P("sp", "tp"),
            P("tp"),
            P(None, "tp"),
            P("sp", "tp"),
            P("sp", "tp"),
            P("sp", "tp"),
            P("sp", None),
            P("sp", None),
            P("sp", None, "tp"),
            P("sp", None, "tp"),
            P("sp", "tp", None),
        ),
        out_specs=(
            P("sp", "tp"),
            P("sp", "tp"),
            P("sp", None, "tp"),
            P("sp", None, "tp"),
            P("sp", "tp", None),
        ),
        check_vma=False,
    )
```

profile of v0, /device:TPU:1, one launch (start us, length us, event | category | flops | bytes accessed | tf_op | source)
XLA Modules:
  0.0 304.2 jit_solution(11217218400964578117)
XLA Ops:
  7.2 0.7 convert_reduce_fusion.3
  7.9 0.1 fusion.78
  8.1 0.7 select_reduce_fusion
  8.8 0.7 convert_add_fusion
  9.5 0.5 convolution_convert_fusion.2
  10.0 0.2 reshape.94
  10.2 1.6 broadcast_in_dim.15
  11.7 12.0 %all-to-all-start.1 = ((bf16[64,12,1024]{2,1,0:T(8,128)(2,1)}), bf16[64,12,1024]{2,1,0:T(8,128)(2,1)S(1)}, u32[]{:S(2)}, u32[]{:S(2)}) async-start(bf16[64,12,1024]{2,1,0:T(8,128)(2,1)} %bitcast.8), calls=%async_computation.1 | async-start | bytes 4194304 | tf_op jit(solution)/shard_map/all_to_all | solution.py:112
  23.8 1.4 convolution_convert_fusion.1
  25.1 1.2 reshape.96
  26.4 25.8 %all-to-all-done.1 = bf16[64,12,1024]{2,1,0:T(8,128)(2,1)S(1)} async-done(((bf16[64,12,1024]{2,1,0:T(8,128)(2,1)}), bf16[64,12,1024]{2,1,0:T(8,128)(2,1)S(1)}, u32[]{:S(2)}, u32[]{:S(2)}) %all-to-all-start.1) | async-done | bytes 1572896 | tf_op jit(solution)/shard_map/all_to_all | solution.py:112
  52.2 0.3 broadcast_in_dim.16
  52.4 35.4 %all_to_all.36 = bf16[64,12,1024]{2,1,0:T(8,128)(2,1)S(1)} all-to-all(bf16[64,12,1024]{2,1,0:T(8,128)(2,1)S(1)} %bitcast.110), channel_id=1, replica_groups=mesh['sp'=64,'tp'=2] {'sp'}, dimensions={0} | all-to-all | bytes 3145728 | tf_op jit(solution)/shard_map/all_to_all | solution.py:113
  87.9 2.4 pad_maximum_fusion
  90.3 0.7 copy-done.14
  91.0 0.1 add_reduce_fusion
  91.1 0.1 convert_element_type.102
  91.3 0.6 copy.36
  91.9 7.2 %all-to-all-start = ((bf16[64,1,12]{2,1,0:T(2,128)(2,1)}), bf16[64,1,12]{2,1,0:T(2,128)(2,1)S(1)}, u32[]{:S(2)}, u32[]{:S(2)}) async-start(bf16[64,1,12]{2,1,0:T(2,128)(2,1)} %copy.36), calls=%async_computation | async-start | bytes 65536 | tf_op jit(solution)/shard_map/all_to_all | solution.py:114
  99.2 0.7 all-gather.13.cloned.1.call-update
  99.9 7.6 %all-to-all-done = bf16[64,1,12]{2,1,0:T(2,128)(2,1)S(1)} async-done(((bf16[64,1,12]{2,1,0:T(2,128)(2,1)}), bf16[64,1,12]{2,1,0:T(2,128)(2,1)S(1)}, u32[]{:S(2)}, u32[]{:S(2)}) %all-to-all-start) | async-done | bytes 1568 | tf_op jit(solution)/shard_map/all_to_all | solution.py:114
  107.5 0.1 convert_reduce_fusion.2
  107.6 0.1 reshape.105
  107.7 4.4 %all-gather.11.cloned.1.call-done = bf16[128,12,2048]{2,1,0:T(8,128)(2,1)} async-done(((bf16[128,12,1024]{2,1,0:T(8,128)(2,1)}), bf16[128,12,2048]{2,1,0:T(8,128)(2,1)}) %all-gather.11.cloned.1.call-update) | async-done | bytes 6291472 | tf_op jit(solution)/shard_map/all_gather | solution.py:12
  112.1 6.3 %fusion.82 = (bf16[64,12,2048]{2,1,0:T(8,128)(2,1)}, bf16[64,12,2048]{2,1,0:T(8,128)(2,1)}) fusion(bf16[128,12,2048]{2,1,0:T(8,128)(2,1)} %all-gather.11.cloned.1.call-done), kind=kLoop, calls=%fused_computation.144 | loop fusion | bytes 12582912 | tf_op jit(solution)/shard_map/split | solution.py:13
  118.4 4.7 %reshape.99 = bf16[768,2048]{1,0:T(8,128)(2,1)S(1)} reshape(bf16[64,12,2048]{2,1,0:T(8,128)(2,1)} %get-tuple-element.10) | data formatting | bytes 6291456 | tf_op jit(solution)/shard_map/reshape | solution.py:120
  123.1 8.1 %fusion.6 = f32[768,896]{1,0:T(8,128)} fusion(bf16[768,2048]{1,0:T(8,128)(2,1)S(1)} %reshape.99, bf16[1,2048,896]{2,1,0:T(8,128)(2,1)} %param.20), kind=kOutput, calls=%fused_computation.10 | convolution fusion | flops 2818572288 | bytes 9568256 | tf_op jit(solution)/shard_map/dot_general | solution.py:127
  131.3 6.2 %reshape.98 = bf16[768,2048]{1,0:T(8,128)(2,1)} reshape(bf16[64,12,2048]{2,1,0:T(8,128)(2,1)} %get-tuple-element.9) | data formatting | bytes 6291456 | tf_op jit(solution)/shard_map/reshape | solution.py:121
  137.4 6.6 %fusion.8 = f32[768,896]{1,0:T(8,128)S(1)} fusion(bf16[768,2048]{1,0:T(8,128)(2,1)} %reshape.98, bf16[1,896,2048]{2,1,0:T(8,128)(2,1)} %param.21), kind=kOutput, calls=%fused_computation.12 | convolution fusion | flops 2818572288 | bytes 9568256 | tf_op jit(solution)/shard_map/dot_general | solution.py:77
  144.1 5.9 %multiply_convert_fusion.1 = (bf16[768,896]{1,0:T(8,128)(2,1)S(1)}, bf16[768,896]{1,0:T(8,128)(2,1)S(1)}, f32[768,896]{1,0:T(8,128)}) fusion(f32[768,896]{1,0:T(8,128)S(1)} %fusion.8, f32[768]{0:T(1024)S(1)} %reshape.105, f32[768,896]{1,0:T(8,128)S(1)} %copy-done.18, bf16[768,2048]{1,0:T(8,128)(2,1)S(1)} %reshape.99, bf16[1,2048,896]{2,1,0:T(8,128)(2,1)S(1)} %copy-done.15), kind=kOutput, calls=%fused_computation.19 | convolution fusion | flops 2828206080 | bytes 17828864 | tf_op jit(solution)/shard_map/dot_general | solution.py:126
  150.0 3.4 %fusion = f32[768,2048]{1,0:T(8,128)S(1)} fusion(bf16[768,896]{1,0:T(8,128)(2,1)S(1)} %get-tuple-element.12, bf16[1,2048,896]{2,1,0:T(8,128)(2,1)S(1)} %copy-done.15), kind=kOutput, calls=%fused_computation.4 | convolution fusion | flops 2818572288 | bytes 11337728 | tf_op jit(solution)/shard_map/dot_general | solution.py:77
  153.4 3.7 %add_convert_fusion = bf16[768,2048]{1,0:T(8,128)(2,1)S(1)} fusion(f32[768,2048]{1,0:T(8,128)S(1)} %fusion, bf16[768,896]{1,0:T(8,128)(2,1)S(1)} %get-tuple-element.11, bf16[1,2048,896]{2,1,0:T(8,128)(2,1)S(1)} %copy-done.16), kind=kOutput, calls=%fused_computation.1 | convolution fusion | flops 2821718016 | bytes 14483456 | tf_op jit(solution)/shard_map/dot_general | solution.py:77
  157.1 0.3 copy.45
  157.5 18.8 %all_to_all.37 = bf16[2,768,1024]{2,1,0:T(8,128)(2,1)S(1)} all-to-all(bf16[2,768,1024]{2,1,0:T(8,128)(2,1)S(1)} %bitcast.108), channel_id=1, replica_groups=mesh['sp'=64,'tp'=2] {'tp'}, dimensions={0} | all-to-all | bytes 6291456 | tf_op jit(solution)/shard_map/all_to_all | solution.py:23
  176.3 2.3 reduce_sum.127
  178.6 3.6 %reshape.101 = bf16[64,12,1024]{2,1,0:T(8,128)(2,1)} reshape(bf16[768,1024]{1,0:T(8,128)(2,1)} %reduce_sum.127) | data formatting | bytes 3145728 | tf_op jit(solution)/shard_map/reshape | solution.py:142
  182.2 10.2 %all-to-all-start.4 = ((bf16[64,12,1024]{2,1,0:T(8,128)(2,1)}), bf16[64,12,1024]{2,1,0:T(8,128)(2,1)S(1)}, u32[]{:S(2)}, u32[]{:S(2)}) async-start(bf16[64,12,1024]{2,1,0:T(8,128)(2,1)} %reshape.101), calls=%async_computation.4 | async-start | bytes 4194304 | tf_op jit(solution)/shard_map/all_to_all | solution.py:141
  192.5 0.1 fusion.18
  192.6 2.0 all-gather.4
  194.7 1.8 all-gather.5
  196.5 0.5 add_rsqrt_fusion
  197.1 0.6 fusion.83
  197.7 23.9 %all-to-all-done.4 = bf16[64,12,1024]{2,1,0:T(8,128)(2,1)S(1)} async-done(((bf16[64,12,1024]{2,1,0:T(8,128)(2,1)}), bf16[64,12,1024]{2,1,0:T(8,128)(2,1)S(1)}, u32[]{:S(2)}, u32[]{:S(2)}) %all-to-all-start.4) | async-done | bytes 1572896 | tf_op jit(solution)/shard_map/all_to_all | solution.py:141
  221.6 1.2 slice_bitcast_fusion
  222.8 1.4 reshape_squeeze.6
  224.2 0.2 reshape_squeeze.7
  224.4 0.3 fusion.74
  224.7 0.4 fusion.17
  225.1 0.2 copy.40
  225.3 5.7 %all_to_all.38 = bf16[2,128,1024]{1,2,0:T(8,128)(2,1)S(1)} all-to-all(bf16[2,128,1024]{1,2,0:T(8,128)(2,1)S(1)} %broadcast_in_dim.17), channel_id=1, replica_groups=mesh['sp'=64,'tp'=2] {'tp'}, dimensions={0} | all-to-all | bytes 1048576 | tf_op jit(solution)/shard_map/all_to_all | solution.py:33
  231.1 3.3 %convolution_convert_fusion = bf16[2048,1024]{1,0:T(8,128)(2,1)} fusion(bf16[128,2048]{0,1:T(8,128)(2,1)S(1)} %bitcast.111, bf16[128,1024]{1,0:T(8,128)(2,1)S(1)} %copy-done.4, f32[1024]{0:T(1024)S(1)} %copy-done.11, f32[128]{0:T(128)S(1)} %copy-done.10, f32[128]{0:T(128)S(1)} %copy-done.9), kind=kOutput, calls=%fused_computation.3 | convolution fusion | flops 540147712 | bytes 4985856 | tf_op jit(solution)/shard_map/dot_general | solution.py:71
  234.4 5.7 %all-to-all-start.6 = ((bf16[64,32,1024]{2,1,0:T(8,128)(2,1)}), bf16[64,32,1024]{2,1,0:T(8,128)(2,1)}, u32[]{:S(2)}, u32[]{:S(2)}) async-start(bf16[64,32,1024]{2,1,0:T(8,128)(2,1)} %bitcast.107), calls=%async_computation.6 | async-start | bytes 8388608 | tf_op jit(solution)/shard_map/all_to_all | solution.py:23
  240.2 7.8 %convert_bitcast_fusion.1 = bf16[1,2048,896]{2,1,0:T(8,128)(2,1)} fusion(bf16[768,2048]{1,0:T(8,128)(2,1)} %copy-done.2, bf16[768,896]{1,0:T(8,128)(2,1)} %copy-done.20), kind=kOutput, calls=%fused_computation.15 | convolution fusion | flops 2820407296 | bytes 8192000 | tf_op jit(solution)/shard_map/dot_general | solution.py:71
  247.9 5.2 %convert_bitcast_fusion = bf16[1,896,2048]{2,1,0:T(8,128)(2,1)} fusion(bf16[768,2048]{1,0:T(8,128)(2,1)S(1)} %copy-done.3, f32[768,896]{1,0:T(8,128)S(1)} %copy-done.19, f32[768,896]{1,0:T(8,128)S(1)} %copy-done.21, f32[768]{0:T(1024)S(1)} %copy-done.13), kind=kOutput, calls=%fused_computation.14 | convolution fusion | flops 2825224192 | bytes 12323840 | tf_op jit(solution)/shard_map/dot_general | solution.py:71
  253.1 3.2 %fusion.81 = (f32[128]{0:T(128)S(1)}, f32[128]{0:T(128)S(1)}, f32[128,1024]{1,0:T(8,128)S(1)}) fusion(f32[128]{0:T(128)S(1)} %copy-done.9, f32[128]{0:T(128)S(1)} %copy-done.10, bf16[128,1024]{1,0:T(8,128)(2,1)S(1)} %copy-done.4, f32[1024]{0:T(1024)S(1)} %copy-done.11, bf16[128,2048]{0,1:T(8,128)(2,1)S(1)} %bitcast.112, ...), kind=kOutput, calls=%fused_computation.143 | convolution fusion | flops 538967808 | bytes 5511168 | tf_op jit(solution)/shard_map/dot_general | solution.py:174
  256.3 2.1 all-gather.6
  258.4 1.8 all-gather.7
  260.2 0.3 fusion.35
  260.5 1.3 collective-permute-start
  261.8 7.6 %convert_bitcast_fusion.2 = bf16[1,2048,896]{2,1,0:T(8,128)(2,1)} fusion(bf16[768,2048]{1,0:T(8,128)(2,1)} %copy-done.2, bf16[768,896]{1,0:T(8,128)(2,1)} %copy-done.17), kind=kOutput, calls=%fused_computation.16 | convolution fusion | flops 2820407296 | bytes 8192000 | tf_op jit(solution)/shard_map/dot_general | solution.py:71
  269.4 20.3 %collective-permute-done = bf16[30,1024]{1,0:T(8,128)(2,1)S(1)} collective-permute-done((bf16[30,1024]{1,0:T(8,128)(2,1)S(1)}, bf16[30,1024]{1,0:T(8,128)(2,1)S(1)}, u32[]{:S(2)}, u32[]{:S(2)}) %collective-permute-start) | collective-permute-done | bytes 61472 | tf_op jit(solution)/shard_map/ppermute | solution.py:52
  289.7 2.7 fusion.37
  292.5 1.0 all-to-all-done.6
  293.5 3.7 %convert_reduce_fusion = f32[32,1024]{1,0:T(8,128)} fusion(bf16[64,32,1024]{2,1,0:T(8,128)(2,1)} %all-to-all-done.6), kind=kLoop, calls=%fused_computation | loop fusion | flops 4161536 | bytes 4325376 | tf_op jit(solution)/shard_map/reduce_sum | solution.py:24
  (59 shorter events, 0.5 us)
Async XLA Ops:
  7.2 2.3 copy-start
  10.1 13.6 %copy-start.5 = (bf16[128,1024]{1,0:T(8,128)(2,1)S(1)}, bf16[128,1024]{1,0:T(8,128)(2,1)}, u32[]{:S(2)}) copy-start(bf16[128,1024]{1,0:T(8,128)(2,1)} %param.16) | copy-start | bytes 786436
  11.7 40.4 %all-to-all-start.1 = ((bf16[64,12,1024]{2,1,0:T(8,128)(2,1)}), bf16[64,12,1024]{2,1,0:T(8,128)(2,1)S(1)}, u32[]{:S(2)}, u32[]{:S(2)}) async-start(bf16[64,12,1024]{2,1,0:T(8,128)(2,1)} %bitcast.8), calls=%async_computation.1 | async-start | bytes 4194304 | tf_op jit(solution)/shard_map/all_to_all | solution.py:112
  23.7 88.4 %all-gather.11.cloned.1.call-start = ((), (), s32[]{:S(2)}) async-start(), calls=%async_computation.7 | async-start | bytes 12582912 | tf_op jit(solution)/shard_map/all_gather | solution.py:12
  90.3 0.7 copy-start.14
  91.9 15.6 %all-to-all-start = ((bf16[64,1,12]{2,1,0:T(2,128)(2,1)}), bf16[64,1,12]{2,1,0:T(2,128)(2,1)S(1)}, u32[]{:S(2)}, u32[]{:S(2)}) async-start(bf16[64,1,12]{2,1,0:T(2,128)(2,1)} %copy.36), calls=%async_computation | async-start | bytes 65536 | tf_op jit(solution)/shard_map/all_to_all | solution.py:114
  99.1 154.0 %all-gather.13.cloned.1.call-start = ((), (), s32[]{:S(2)}) async-start(), calls=%async_computation.8 | async-start | bytes 4259840 | tf_op jit(solution)/shard_map/all_gather | solution.py:176
  107.7 36.3 %copy-start.12 = (f32[768]{0:T(1024)}, f32[768]{0:T(1024)S(1)}, u32[]{:S(2)}) copy-start(f32[768]{0:T(1024)S(1)} %reshape.105) | copy-start | bytes 9220
  123.1 20.9 %copy-start.2 = (bf16[768,2048]{1,0:T(8,128)(2,1)}, bf16[768,2048]{1,0:T(8,128)(2,1)S(1)}, u32[]{:S(2)}) copy-start(bf16[768,2048]{1,0:T(8,128)(2,1)S(1)} %reshape.99) | copy-start | bytes 9437188
  137.4 6.6 %copy-start.15 = (bf16[1,2048,896]{2,1,0:T(8,128)(2,1)S(1)}, bf16[1,2048,896]{2,1,0:T(8,128)(2,1)}, u32[]{:S(2)}) copy-start(bf16[1,2048,896]{2,1,0:T(8,128)(2,1)} %param.19) | copy-start | bytes 11010052
  137.4 6.6 %copy-start.18 = (f32[768,896]{1,0:T(8,128)S(1)}, f32[768,896]{1,0:T(8,128)}, u32[]{:S(2)}) copy-start(f32[768,896]{1,0:T(8,128)} %fusion.6) | copy-start | bytes 8257540
  150.0 3.5 %copy-start.17 = (bf16[768,896]{1,0:T(8,128)(2,1)}, bf16[768,896]{1,0:T(8,128)(2,1)S(1)}, u32[]{:S(2)}) copy-start(bf16[768,896]{1,0:T(8,128)(2,1)S(1)} %get-tuple-element.12) | copy-start | bytes 4128772
  150.0 3.5 %copy-start.20 = (bf16[768,896]{1,0:T(8,128)(2,1)}, bf16[768,896]{1,0:T(8,128)(2,1)S(1)}, u32[]{:S(2)}) copy-start(bf16[768,896]{1,0:T(8,128)(2,1)S(1)} %get-tuple-element.11) | copy-start | bytes 4128772
  150.0 3.5 %copy-start.16 = (bf16[1,2048,896]{2,1,0:T(8,128)(2,1)S(1)}, bf16[1,2048,896]{2,1,0:T(8,128)(2,1)}, u32[]{:S(2)}) copy-start(bf16[1,2048,896]{2,1,0:T(8,128)(2,1)} %param.20) | copy-start | bytes 11010052
  178.6 13.9 %copy-start.4 = (bf16[128,1024]{1,0:T(8,128)(2,1)S(1)}, bf16[128,1024]{1,0:T(8,128)(2,1)}, u32[]{:S(2)}) copy-start(bf16[128,1024]{1,0:T(8,128)(2,1)} %param.11) | copy-start | bytes 786436
  182.2 14.8 %copy-start.7 = (bf16[31,1024]{1,0:T(8,128)(2,1)S(1)}, bf16[31,1024]{1,0:T(8,128)(2,1)}, u32[]{:S(2)}) copy-start(bf16[31,1024]{1,0:T(8,128)(2,1)} %param.13) | copy-start | bytes 190468
  182.2 39.4 %all-to-all-start.4 = ((bf16[64,12,1024]{2,1,0:T(8,128)(2,1)}), bf16[64,12,1024]{2,1,0:T(8,128)(2,1)S(1)}, u32[]{:S(2)}, u32[]{:S(2)}) async-start(bf16[64,12,1024]{2,1,0:T(8,128)(2,1)} %reshape.101), calls=%async_computation.4 | async-start | bytes 4194304 | tf_op jit(solution)/shard_map/all_to_all | solution.py:141
  222.8 1.9 copy-start.6
  224.4 6.7 %copy-start.9 = (f32[128]{0:T(128)S(1)}, f32[128]{0:T(128)}, u32[]{:S(2)}) copy-start(f32[128]{0:T(128)} %get-tuple-element.50) | copy-start | bytes 1540
  224.4 6.7 %copy-start.10 = (f32[128]{0:T(128)S(1)}, f32[128]{0:T(128)}, u32[]{:S(2)}) copy-start(f32[128]{0:T(128)} %get-tuple-element.51) | copy-start | bytes 1540
  224.4 6.7 %copy-start.11 = (f32[1024]{0:T(1024)S(1)}, f32[1024]{0:T(1024)}, u32[]{:S(2)}) copy-start(f32[1024]{0:T(1024)} %param.12) | copy-start | bytes 12292
  234.4 59.1 %all-to-all-start.6 = ((bf16[64,32,1024]{2,1,0:T(8,128)(2,1)}), bf16[64,32,1024]{2,1,0:T(8,128)(2,1)}, u32[]{:S(2)}, u32[]{:S(2)}) async-start(bf16[64,32,1024]{2,1,0:T(8,128)(2,1)} %bitcast.107), calls=%async_computation.6 | async-start | bytes 8388608 | tf_op jit(solution)/shard_map/all_to_all | solution.py:23
  240.1 7.8 %copy-start.3 = (bf16[768,2048]{1,0:T(8,128)(2,1)S(1)}, bf16[768,2048]{1,0:T(8,128)(2,1)}, u32[]{:S(2)}) copy-start(bf16[768,2048]{1,0:T(8,128)(2,1)} %reshape.98) | copy-start | bytes 9437188
  240.1 7.8 %copy-start.13 = (f32[768]{0:T(1024)S(1)}, f32[768]{0:T(1024)}, u32[]{:S(2)}) copy-start(f32[768]{0:T(1024)} %copy-done.12) | copy-start | bytes 9220
  240.1 7.8 %copy-start.19 = (f32[768,896]{1,0:T(8,128)S(1)}, f32[768,896]{1,0:T(8,128)}, u32[]{:S(2)}) copy-start(f32[768,896]{1,0:T(8,128)} %fusion.6) | copy-start | bytes 8257540
  240.1 7.8 %copy-start.21 = (f32[768,896]{1,0:T(8,128)S(1)}, f32[768,896]{1,0:T(8,128)}, u32[]{:S(2)}) copy-start(f32[768,896]{1,0:T(8,128)} %get-tuple-element.52) | copy-start | bytes 8257540
  260.5 29.3 %copy-start.8 = (f32[1,1024]{1,0:T(1,128)S(1)}, f32[1,1024]{1,0:T(1,128)}, u32[]{:S(2)}) copy-start(f32[1,1024]{1,0:T(1,128)} %get-tuple-element.33) | copy-start | bytes 12292
  260.5 29.2 %collective-permute-start = (bf16[30,1024]{1,0:T(8,128)(2,1)S(1)}, bf16[30,1024]{1,0:T(8,128)(2,1)S(1)}, u32[]{:S(2)}, u32[]{:S(2)}) collective-permute-start(bf16[30,1024]{1,0:T(8,128)(2,1)S(1)} %slice.279), channel_id=1, source_target_pairs={{2,0},{4,2},{6,4},{8,6},{10,8},{12,10},{14,12},{16,14},{18,16},{20... | collective-permute-start | bytes 184328 | tf_op jit(solution)/shard_map/ppermute | solution.py:52
  289.7 7.5 %copy-start.1 = (bf16[128,1024]{1,0:T(8,128)(2,1)S(1)}, bf16[128,1024]{1,0:T(8,128)(2,1)}, u32[]{:S(2)}) copy-start(bf16[128,1024]{1,0:T(8,128)(2,1)} %param.15) | copy-start | bytes 786436
Sparse Core Ops, SparseCore 0:
  90.4 21.6 all-gather.10
  115.0 68.3 all-gather.12
where the time goes:
time: 305 us; the launch traced here: 304 us
  waiting for transfers between devices  83.7 us (27%)
  blocking collectives  67.7 us (22%)
  matrix products  57.4 us (19%)
  starting transfers between devices  36.5 us (12%)
  local copies, waits for them, and re-layouts  29.7 us (10%)
  between operations  14.7 us (5%)
  other arithmetic  14.6 us (5%)
    all_to_all x1, blocking collectives, on_device(): lax.all_to_all(packed(out_grad), 'sp', split_axis=0, concat_axis=0, tiled...  35.4 us
    all_to_all x1, waiting for transfers between devices, on_device(): lax.all_to_all(packed(stream_mid), 'sp', split_axis=0, concat_axis=0, til...  25.8 us
    dot_general x6, matrix products, contract_rows(): lax.dot_general(left, right, (((0,), (0,)), ((), ())), preferred_element_...  25.7 us
    all_to_all x1, waiting for transfers between devices, on_device(): lax.all_to_all(summed.reshape(arrived_mid.shape[0], capacity, summed.shap...  23.9 us
    ppermute x1, waiting for transfers between devices, passed_along(): lax.ppermute(value, axis, [(source, source + steps) for source in range(f...  20.3 us
    all_to_all x1, blocking collectives, summed_on_arrival(): lax.all_to_all(blocks, axis, split_axis=0, concat_axis=0, tiled=True)  18.8 us
    dot_general x3, matrix products, contract_cols(): lax.dot_general(left, right, (((1,), (1,)), ((), ())), preferred_element_...  13.7 us
    all_to_all x1, starting transfers between devices, on_device(): lax.all_to_all(packed(stream_mid), 'sp', split_axis=0, concat_axis=0, til...  12 us
  transfers between devices with their start and end apart: 7, of which 6 were waited for; matrix products, arithmetic and copies ran while one was open for 30% of the time, Pallas kernels for 0%

commit v1 on v0

v1 whole, which is shorter than its diff:
```python
import functools

import jax
import jax.numpy as jnp
from jax import lax
from jax.experimental import pallas as pl
from jax.experimental.pallas import tpu as pltpu
from jax.sharding import PartitionSpec as P

D = 2048
HALF = 1024
MAIN = 8
REM = 4
MESH = pl.DeviceIdType.MESH
F32 = jnp.float32
BF16 = jnp.bfloat16


def nt(a, b):
    return lax.dot_general(a, b, (((1,), (1,)), ((), ())), preferred_element_type=F32)


def nn(a, b):
    return lax.dot_general(a, b, (((1,), (0,)), ((), ())), preferred_element_type=F32)


def tn(a, b):
    return lax.dot_general(a, b, (((0,), (0,)), ((), ())), preferred_element_type=F32)


def sp_copy(src, dst, send, recv, sp):
    return pltpu.make_async_remote_copy(
        src_ref=src, dst_ref=dst, send_sem=send, recv_sem=recv,
        device_id={"sp": sp}, device_id_type=MESH,
    )


def tp_copy(src, dst, send, recv, tp):
    return pltpu.make_async_remote_copy(
        src_ref=src, dst_ref=dst, send_sem=send, recv_sem=recv,
        device_id={"tp": tp}, device_id_type=MESH,
    )


def gray(k):
    return lax.rem(k + k // 2 - 2 * (k // 3), 4)


def expert_kernel(
    pk, wg_hbm, wu_hbm, wd_hbm,
    xs_out, ps_out, a_out, dg_out, du_out, ret_out,
    wg, wu, wd, own, oth, xs, ps, acts, dgs, dus,
    psend, precv, pown, rsend, ret,
    sel_a, sel_b,
    w_sem, a_send, b_send, c_send, own_sem, oth_sem,
    e_send, e_recv, r_send, r_recv, o_sem,
):
    me = lax.axis_index("sp")
    tp = lax.axis_index("tp")
    peer = 1 - tp
    mx, my, mz = lax.rem(me, 4), lax.rem(me // 4, 4), me // 16
    twin = me + 1 - 2 * lax.rem(me, 2)
    loads = [
        pltpu.make_async_copy(src, dst, w_sem.at[i])
        for i, (src, dst) in enumerate(((wg_hbm, wg), (wu_hbm, wu), (wd_hbm, wd)))
    ]
    for copy in loads:
        copy.start()

    barrier = pltpu.get_barrier_semaphore()

    def greet(k, _):
        pl.semaphore_signal(
            barrier, inc=1, device_id={"sp": lax.rem(me + k, 64)}, device_id_type=MESH
        )
        return 0

    lax.fori_loop(1, 64, greet, 0)
    pl.semaphore_signal(barrier, inc=1, device_id={"tp": peer}, device_id_type=MESH)

    row = lax.broadcasted_iota(jnp.int32, (64, 128), 0)
    col = lax.broadcasted_iota(jnp.int32, (64, 128), 1)
    spot = (row // 4) * 8 + row % 4
    sel_a[...] = (col == spot).astype(F32).astype(BF16)
    sel_b[...] = (col == spot + 4).astype(F32).astype(BF16)
    own[pl.ds(me, 1)] = pk[pl.ds(me // 2, 1)]

    pl.semaphore_wait(barrier, 64)

    def direct_send(i):
        k, j = i // 8, lax.rem(i, 8)
        dz, dy, side = gray(k), gray(j // 2), lax.rem(j, 2)
        x = mx + side * (3 - 2 * mx)
        to = lax.rem(mz + dz, 4) * 16 + lax.rem(my + dy, 4) * 4 + x
        return sp_copy(pk.at[to // 2], own.at[me], a_send.at[i], own_sem.at[me], to)

    def start_direct(i, _):
        direct_send(i).start()
        return 0

    lax.fori_loop(1, 32, start_direct, 0)

    def source(k, j, near):
        dz, dy, side = gray(k), gray(j // 2), lax.rem(j, 2)
        x = mx + side * (3 - 2 * mx)
        twin_x = x + 1 - 2 * lax.rem(x, 2)
        x = x if near else twin_x
        return lax.rem(mz - dz + 4, 4) * 16 + lax.rem(my - dy + 4, 4) * 4 + x

    def twin_copy(i):
        s = source(i // 8, lax.rem(i, 8), True)
        return sp_copy(own.at[s], own.at[s], b_send.at[i], own_sem.at[s], twin)

    def core_copy(s):
        return tp_copy(own.at[s], oth.at[s], c_send.at[s], oth_sem.at[s], peer)

    def arrived(s):
        return sp_copy(own.at[s], own.at[s], c_send.at[s], own_sem.at[s], twin)

    def take_direct(k):
        def one(j, _):
            s = source(k, j, True)

            @pl.when(k * 8 + j != 0)
            def _():
                arrived(s).wait_recv()

            twin_copy(k * 8 + j).start()
            core_copy(s).start()
            return 0

        lax.fori_loop(0, 8, one, 0)

    def take_twin(k):
        def one(j, _):
            s = source(k, j, False)
            arrived(s).wait_recv()
            core_copy(s).start()
            return 0

        lax.fori_loop(0, 8, one, 0)

    def part_copy(z):
        return tp_copy(
            psend.at[pl.ds(z * 16, 16)], precv.at[pl.ds(z * 16, 16)],
            e_send.at[z], e_recv.at[z], peer,
        )

    def ret_copy(s):
        return sp_copy(rsend.at[s], ret.at[me], r_send.at[s], r_recv.at[me], s)

    def ret_arrived(s):
        return sp_copy(rsend.at[s], ret.at[s], r_send.at[s], r_recv.at[s], s)

    def plane(k):
        return lax.rem(mz - gray(k) + 4, 4)

    def compute(k):
        z = plane(k)

        def wait_other(j, _):
            tp_copy(
                own.at[z * 16 + j], oth.at[z * 16 + j],
                c_send.at[z * 16 + j], oth_sem.at[z * 16 + j], peer,
            ).wait_recv()
            return 0

        lax.fori_loop(0, 16, wait_other, 0)
        base = pl.multiple_of(z * 192, 64)
        for buf, half in ((own, tp), (oth, peer)):
            block = buf[pl.ds(z * 16, 16)].reshape(128, 3072)
            left = pl.multiple_of(half * HALF, HALF)
            mid = pl.multiple_of(half * HALF + 512, 512)
            xs[pl.ds(base, 128), pl.ds(left, HALF)] = block[:, :HALF]
            ps[pl.ds(base, 128), pl.ds(left, HALF)] = block[:, HALF : 2 * HALF]
            rest = block[:, 2 * HALF :]
            first = nn(sel_a[...], rest).astype(BF16)
            second = nn(sel_b[...], rest).astype(BF16)
            low = pl.multiple_of(base + 128, 64)
            xs[pl.ds(low, 64), pl.ds(left, 512)] = first[:, :512]
            xs[pl.ds(low, 64), pl.ds(mid, 512)] = second[:, :512]
            ps[pl.ds(low, 64), pl.ds(left, 512)] = first[:, 512:]
            ps[pl.ds(low, 64), pl.ds(mid, 512)] = second[:, 512:]
        x = xs[pl.ds(base, 192), :]
        p = ps[pl.ds(base, 192), :]
        g = nn(x, wg[...])
        u = nn(x, wu[...])
        dh = nt(p, wd[...])
        sig = jax.nn.sigmoid(g)
        silu = g * sig
        acts[pl.ds(base, 192), :] = (silu * u).astype(BF16)
        dg = (dh * u * sig * (1.0 + g * (1.0 - sig))).astype(BF16)
        du = (dh * silu).astype(BF16)
        dgs[pl.ds(base, 192), :] = dg
        dus[pl.ds(base, 192), :] = du
        for out, half in ((psend, peer), (pown, tp)):
            rows = pl.ds(pl.multiple_of(half * HALF, HALF), HALF)
            back = nt(dg, wg[rows, :]) + nt(du, wu[rows, :])
            back = back.astype(BF16)
            out[pl.ds(z * 16, 16), :, :HALF] = back[:128].reshape(16, 8, HALF)
            rest = tn(sel_a[...], back[128:, :512]) + tn(sel_b[...], back[128:, 512:])
            out[pl.ds(z * 16, 16), :, HALF:] = rest.astype(BF16).reshape(16, 8, 512)
            if half is peer:
                part_copy(z).start()

    def give_back(k):
        z = plane(k)
        part_copy(z).wait_recv()
        block = pl.ds(z * 16, 16)
        rsend[block] = (pown[block].astype(F32) + precv[block].astype(F32)).astype(BF16)

        def one(j, _):
            s = z * 16 + lax.rem(lax.rem(me, 16) + j, 16)

            @pl.when(s != me)
            def _():
                ret_copy(s).start()

            return 0

        lax.fori_loop(0, 16, one, 0)

    take_direct(0)
    take_direct(1)
    take_twin(0)
    for copy in loads:
        copy.wait()

    def step(k, _):
        @pl.when(k < 2)
        def _():
            take_direct(k + 2)

        compute(k)

        @pl.when(k < 3)
        def _():
            take_twin(k + 1)

        @pl.when(k > 0)
        def _():
            give_back(k - 1)

        return 0

    lax.fori_loop(0, 4, step, 0)
    outs = [
        pltpu.make_async_copy(src, dst, o_sem.at[i])
        for i, (src, dst) in enumerate(
            ((xs, xs_out), (ps, ps_out), (acts, a_out), (dgs, dg_out), (dus, du_out))
        )
    ]
    for copy in outs:
        copy.start()
    give_back(3)
    ret[pl.ds(me, 1)] = rsend[pl.ds(me, 1)]

    def finish_sends(i, _):
        @pl.when(i > 0)
        def _():
            direct_send(i).wait_send()

        twin_copy(i).wait_send()
        return 0

    lax.fori_loop(0, 32, finish_sends, 0)

    def finish(s, _):
        core_copy(s).wait_send()

        @pl.when(s != me)
        def _():
            ret_copy(s).wait_send()
            ret_arrived(s).wait_recv()

        return 0

    lax.fori_loop(0, 64, finish, 0)
    for z in range(4):
        part_copy(z).wait_send()
    last = pltpu.make_async_copy(ret, ret_out, o_sem.at[5])
    last.start()
    for copy in outs:
        copy.wait()
    last.wait()


def run_experts(pk, wg, wu, wd):
    hidden = wg.shape[1]
    rows = 768
    out = [
        jax.ShapeDtypeStruct((rows, D), BF16),
        jax.ShapeDtypeStruct((rows, D), BF16),
        jax.ShapeDtypeStruct((rows, hidden), BF16),
        jax.ShapeDtypeStruct((rows, hidden), BF16),
        jax.ShapeDtypeStruct((rows, hidden), BF16),
        jax.ShapeDtypeStruct((64, 8, 1536), BF16),
    ]
    dma = pltpu.SemaphoreType.DMA
    return pl.pallas_call(
        expert_kernel,
        out_shape=out,
        in_specs=[pl.BlockSpec(memory_space=pltpu.VMEM)] + [pl.BlockSpec(memory_space=pl.ANY)] * 3,
        out_specs=[pl.BlockSpec(memory_space=pl.ANY)] * 6,
        scratch_shapes=[
            pltpu.VMEM((D, hidden), BF16),
            pltpu.VMEM((D, hidden), BF16),
            pltpu.VMEM((hidden, D), BF16),
            pltpu.VMEM((64, 8, 3072), BF16),
            pltpu.VMEM((64, 8, 3072), BF16),
            pltpu.VMEM((rows, D), BF16),
            pltpu.VMEM((rows, D), BF16),
            pltpu.VMEM((rows, hidden), BF16),
            pltpu.VMEM((rows, hidden), BF16),
            pltpu.VMEM((rows, hidden), BF16),
            pltpu.VMEM((64, 8, 1536), BF16),
            pltpu.VMEM((64, 8, 1536), BF16),
            pltpu.VMEM((64, 8, 1536), BF16),
            pltpu.VMEM((64, 8, 1536), BF16),
            pltpu.VMEM((64, 8, 1536), BF16),
            pltpu.VMEM((64, 128), BF16),
            pltpu.VMEM((64, 128), BF16),
            dma((3,)), dma((32,)), dma((32,)), dma((64,)), dma((64,)), dma((64,)),
            dma((4,)), dma((4,)), dma((64,)), dma((64,)), dma((6,)),
        ],
        compiler_params=pltpu.CompilerParams(
            collective_id=0, has_side_effects=True, vmem_limit_bytes=56 * 1024 * 1024
        ),
        name="experts",
    )(pk, wg, wu, wd)


def slots_of(route_block, experts):
    tok = route_block.shape[0]
    labels = jnp.arange(experts, dtype=jnp.int32)
    onehot = (route_block[:, :, None] == labels[None, None, :]).astype(F32)
    per_token = jnp.sum(onehot, axis=1)
    earlier = (jnp.arange(tok)[:, None] > jnp.arange(tok)[None, :]).astype(F32)
    before = jnp.dot(earlier, per_token)
    return jnp.sum(onehot * before[:, None, :], axis=2).astype(jnp.int32)


def tables(routes, experts):
    slot = slots_of(routes, experts)
    at = jnp.arange(experts * MAIN, dtype=jnp.int32)[None, None, :]
    base = routes * MAIN + slot
    main = (base[:, :, None] == at) & (slot < MAIN)[:, :, None]
    first = (base[:, :, None] - MAIN == at) & (slot >= MAIN)[:, :, None]
    second = (base[:, :, None] - REM == at) & (slot >= MAIN)[:, :, None]
    return main, first, second


def total_of_pieces(array, axis):
    return lax.all_gather(array, axis).sum(0)


def gather_directly(array, axis, dim):
    peers = lax.axis_size(axis)
    blocks = lax.all_to_all(
        jnp.broadcast_to(array[None], (peers, *array.shape)), axis, 0, 0, tiled=True
    )
    shape = list(array.shape)
    shape[dim] *= peers
    return jnp.moveaxis(blocks, 0, dim).reshape(shape)


def summed_on_arrival(array, axis, dim):
    peers = lax.axis_size(axis)
    before, after = array.shape[:dim], array.shape[dim + 1 :]
    blocks = jnp.moveaxis(array.reshape(*before, peers, -1, *after), dim, 0)
    arrived = lax.all_to_all(blocks, axis, split_axis=0, concat_axis=0, tiled=True)
    return arrived.astype(F32).sum(axis=0)


def on_device(
    conv_out, ln_gain, taps, proj_weight, stream_mid, out_grad,
    routes, route_probs, gate_slabs, up_slabs, down_slabs,
):
    tok_rows = conv_out.shape[0]
    experts = lax.axis_size("sp") // 2
    main, first, second = tables(routes, experts)

    def pick(t):
        return (t[:, 0] | t[:, 1]).astype(BF16)

    def weights(t):
        return jnp.sum(t.astype(F32) * route_probs[:, :, None], axis=(0, 1))[:, None]

    s_main, s_first, s_second = pick(main), pick(first), pick(second)
    p_main, p_rest = weights(main), weights(first) + weights(second)
    rest_mid = tn(s_first, stream_mid[:, :512]) + tn(s_second, stream_mid[:, 512:])
    rest_grad = tn(s_first, out_grad[:, :512]) + tn(s_second, out_grad[:, 512:])
    pk = jnp.concatenate(
        [
            tn(s_main, stream_mid).astype(BF16),
            (tn(s_main, out_grad) * p_main).astype(BF16),
            rest_mid.astype(BF16),
            (rest_grad * p_rest).astype(BF16),
        ],
        axis=1,
    ).reshape(experts, MAIN, 3072)

    xs, ps, acts, dg, du, ret = run_experts(pk, gate_slabs[0], up_slabs[0], down_slabs[0])
    grad_down = tn(acts, ps).astype(BF16)
    grad_gate = tn(xs, dg).astype(BF16)
    grad_up = tn(xs, du).astype(BF16)

    pairs = ret.reshape(experts, 2, MAIN, 1536)
    contrib = 0.0
    for h in range(2):
        rows = pairs[:, h].reshape(experts * MAIN, 1536)
        contrib = contrib + nn(s_main, rows[:, :HALF])
        contrib = contrib + jnp.concatenate(
            [nn(s_first, rows[:, HALF:]), nn(s_second, rows[:, HALF:])], axis=1
        )
    grad_stream = (out_grad.astype(F32) + contrib).astype(BF16)

    values = conv_out.astype(F32)
    row_total = total_of_pieces(jnp.sum(values, axis=1), "tp")
    row_squares = total_of_pieces(jnp.sum(values * values, axis=1), "tp")
    row_mean = row_total[:, None] / D
    row_var = row_squares[:, None] / D - row_mean * row_mean
    inv_std = lax.rsqrt(row_var + 1e-06)
    normed = (values - row_mean) * inv_std
    scaled_z = normed * ln_gain[None, :]
    z_sig = jax.nn.sigmoid(scaled_z)
    activated = (scaled_z * z_sig).astype(BF16)
    whole_stream = gather_directly(grad_stream, "tp", 1)
    grad_act = nn(whole_stream, lax.all_gather(proj_weight, "sp", axis=0, tiled=True))
    grad_normed = grad_act * z_sig * (1.0 + scaled_z * (1.0 - z_sig)) * ln_gain[None, :]
    first_sum = total_of_pieces(jnp.sum(grad_normed, axis=1), "tp")
    second_sum = total_of_pieces(jnp.sum(grad_normed * normed, axis=1), "tp")
    grad_conv = (
        inv_std * (grad_normed - first_sum[:, None] / D - normed * second_sum[:, None] / D)
    ).astype(BF16)
    reach = taps.shape[0] - 1
    following = lax.ppermute(grad_conv[:reach], "sp", [(k, k - 1) for k in range(1, 64)])
    extended = jnp.concatenate([grad_conv, following], axis=0).astype(F32)
    tap_values = taps.astype(F32)
    grad_input = jnp.zeros((tok_rows, grad_conv.shape[1]), F32)
    for offset in range(taps.shape[0]):
        grad_input = grad_input + tap_values[offset][None, :] * extended[offset : offset + tok_rows]
    grad_proj = summed_on_arrival(tn(whole_stream, activated).astype(BF16), "sp", 0)
    return (
        grad_input.astype(BF16), grad_proj, grad_gate[None], grad_up[None], grad_down[None],
    )


def solution(mesh):
    return jax.shard_map(
        on_device,
        mesh=mesh,
        in_specs=(
            P("sp", "tp"), P("tp"), P(None, "tp"), P("sp", "tp"), P("sp", "tp"), P("sp", "tp"),
            P("sp", None), P("sp", None), P("sp", None, "tp"), P("sp", None, "tp"), P("sp", "tp", None),
        ),
        out_specs=(
            P("sp", "tp"), P("sp", "tp"), P("sp", None, "tp"), P("sp", None, "tp"), P("sp", "tp", None),
        ),
        check_vma=False,
    )
```

time: 305 us -> 197 us (0.65)
  Pallas kernels: 0 us -> 86.7 us
  blocking collectives: 67.7 us -> 7.31 us
  waiting for transfers between devices: 83.7 us -> 28.8 us
  matrix products: 57.4 us -> 30.1 us
  local copies, waits for them, and re-layouts: 29.7 us -> 2.63 us
  starting transfers between devices: 36.5 us -> 13.9 us
    pallas_call x0 -> x1, Pallas kernels: none -> 86.7 us  [run_experts(): pl.pallas_call(expert_kernel, out_shape=out, in_specs=[pl.BlockSpec(memor...]
    all_to_all x3 -> x0, blocking collectives: 60 us -> none  [the longest x1 35.4 us: on_device(): lax.all_to_all(packed(out_grad), 'sp', split_axis=0, concat_axis=0, tiled...]
    all_to_all x3 -> x1, waiting for transfers between devices: 57.3 us -> 0.01 us  [gather_directly(): lax.all_to_all(jnp.broadcast_to(array[None], (peers, *array.shape)), axis...]
    dot_general x15 -> x18, matrix products: 57.4 us -> 30.1 us  [the longest x10 25.6 us: tn(): lax.dot_general(a, b, (((0,), (0,)), ((), ())), preferred_element_type=F32)]
    all_to_all x1, waiting for transfers between devices: 1.05 us -> 28.1 us  [summed_on_arrival(): lax.all_to_all(blocks, axis, split_axis=0, concat_axis=0, tiled=True)]
    all_to_all x3 -> x1, starting transfers between devices: 29.4 us -> 4.26 us  [gather_directly(): lax.all_to_all(jnp.broadcast_to(array[None], (peers, *array.shape)), axis...]
    ppermute x1, waiting for transfers between devices: 20.3 us -> 0.01 us  [on_device(): lax.ppermute(grad_conv[:reach], 'sp', [(k, k - 1) for k in range(1, 64)])]
    reshape x6 -> x0, local copies, waits for them, and re-layouts: 16.3 us -> none  [the longest x1 6.17 us: on_device(): expert_grad = arrived_grad.reshape(slot_rows, arrived_grad.shape[2])]
  transfers between devices with their start and end apart: 7 -> 4, of which waited for: 6 -> 1; matrix products, arithmetic and copies ran while one was open for 30% -> 21% of each run, Pallas kernels for 0% -> 44%
where the time goes in v1:
time: 197 us; the launch traced here: 196 us
  Pallas kernels  86.7 us (44%)
  matrix products  30.1 us (15%)
  waiting for transfers between devices  28.8 us (15%)
  between operations  14.3 us (7%)
  starting transfers between devices  13.9 us (7%)
  other arithmetic  11.7 us (6%)
  blocking collectives  7.31 us (4%)
  local copies, waits for them, and re-layouts  2.63 us (1%)
    pallas_call x1, Pallas kernels, run_experts(): pl.pallas_call(expert_kernel, out_shape=out, in_specs=[pl.BlockSpec(memor...  86.7 us
    all_to_all x1, waiting for transfers between devices, summed_on_arrival(): lax.all_to_all(blocks, axis, split_axis=0, concat_axis=0, tiled=True)  28.1 us
    dot_general x10, matrix products, tn(): lax.dot_general(a, b, (((0,), (0,)), ((), ())), preferred_element_type=F32)  25.6 us
    all_to_all x1, starting transfers between devices, summed_on_arrival(): lax.all_to_all(blocks, axis, split_axis=0, concat_axis=0, tiled=True)  8.34 us
    all_gather x4, blocking collectives, total_of_pieces(): return lax.all_gather(array, axis).sum(0)  7.31 us
    dot_general x7, matrix products, nn(): lax.dot_general(a, b, (((1,), (0,)), ((), ())), preferred_element_type=F32)  4.4 us
    all_to_all x1, starting transfers between devices, gather_directly(): lax.all_to_all(jnp.broadcast_to(array[None], (peers, *array.shape)), axis...  4.26 us
  transfers between devices with their start and end apart: 4, of which 1 were waited for; matrix products, arithmetic and copies ran while one was open for 21% of the time, Pallas kernels for 44%

profile of v1, /device:TPU:1, one launch (start us, length us, event | category | flops | bytes accessed | tf_op | source)
XLA Modules:
  0.0 195.5 jit_solution(12525237789037181453)
XLA Ops:
  7.2 0.0 copy-start.1
  7.2 0.0 copy-start.2
  7.2 0.0 all-gather.10.cloned.1.call-start
  7.2 0.7 all-gather.10.cloned.1.call-update
  7.9 0.7 convert_reduce_fusion.2
  8.6 0.1 fusion.85
  8.8 0.7 select_reduce_fusion.3
  9.5 0.7 broadcast_add_fusion
  10.2 0.2 fusion.67
  10.5 1.0 select_reduce_fusion
  11.6 1.2 fusion.77
  12.7 1.2 fusion.80
  13.9 1.3 convolution_convert_fusion.1
  15.2 1.3 fusion
  16.5 0.0 copy-done.2
  16.5 0.3 fusion.8
  16.8 0.0 copy-done.1
  16.8 0.3 fusion.6
  17.1 1.3 maximum_bitcast_fusion.pk
  18.4 86.7 %experts.1 = (bf16[768,2048]{1,0:T(8,128)(2,1)}, bf16[768,2048]{1,0:T(8,128)(2,1)}, bf16[768,896]{1,0:T(8,128)(2,1)}, bf16[768,896]{1,0:T(8,128)(2,1)}, bf16[768...) custom-call(bf16[32,8,3072]{2,1,0:T(8,128)(2,1)} %maximum_bitcast_fusion.pk, bf16[2048,896]{1,0:T(8,128)(2,1)} %bitcast.88, ...), custom_call_target="tpu_custom_call" | custom-call | tf_op jit(solution)/shard_map/experts/pallas_call | solution.py:300
  105.1 1.5 slice_bitcast_fusion
  106.5 0.2 fusion.68
  106.7 0.2 fusion.70
  106.9 0.2 fusion.72
  107.1 0.2 fusion.74
  107.3 0.0 copy-start
  107.3 0.0 copy-start.4
  107.3 0.2 convolution_add_fusion.3
  107.6 0.2 fusion.7
  107.8 0.2 copy.30
  108.0 0.8 broadcast_in_dim.8
  108.8 4.3 %all-to-all-start = ((bf16[2,128,1024]{1,2,0:T(8,128)(2,1)}), bf16[2,128,1024]{1,2,0:T(8,128)(2,1)S(1)}, u32[]{:S(2)}, u32[]{:S(2)}) async-start(bf16[2,128,1024]{1,2,0:T(8,128)(2,1)} %broadcast_in_dim.8), calls=%async_computation | async-start | bytes 1048576 | tf_op jit(solution)/shard_map/all_to_all | solution.py:359
  113.1 0.0 copy-done
  113.1 0.1 fusion.9
  113.2 1.8 all-gather.5
  115.1 1.8 all-gather.4
  116.9 0.0 all-to-all-done
  116.9 0.0 copy-done.4
  116.9 3.4 %convolution_convert_fusion = bf16[2048,1024]{1,0:T(8,128)(2,1)} fusion(bf16[128,2048]{0,1:T(8,128)(2,1)S(1)} %bitcast.86, bf16[128,1024]{1,0:T(8,128)(2,1)S(1)} %copy-done, f32[1024]{0:T(1024)S(1)} %copy-done.4, f32[128]{0:T(128)S(1)} %get-tuple-element.62, f32[128]{0:T(128)S(1)} %get-tuple-element.61), kind=kOutput, calls=%fused_computation.1 | convolution fusion | flops 540147712 | bytes 4985856 | tf_op jit(solution)/shard_map/dot_general | solution.py:28
  120.3 0.0 copy-start.3
  120.3 0.0 copy-start.9
  120.3 8.3 %all-to-all-start.1 = ((bf16[64,32,1024]{2,1,0:T(8,128)(2,1)}), bf16[64,32,1024]{2,1,0:T(8,128)(2,1)}, u32[]{:S(2)}, u32[]{:S(2)}) async-start(bf16[64,32,1024]{2,1,0:T(8,128)(2,1)} %bitcast.85), calls=%async_computation.1 | async-start | bytes 8388608 | tf_op jit(solution)/shard_map/all_to_all | solution.py:371
  128.6 0.0 copy-done.3
  128.7 0.1 fusion.88
  128.7 0.0 copy-done.9
  128.8 0.0 copy-start.6
  128.8 0.0 copy-start.8
  128.8 7.4 %convert_bitcast_fusion.2 = bf16[1,2048,896]{2,1,0:T(8,128)(2,1)} fusion(bf16[768,2048]{1,0:T(8,128)(2,1)} %get-tuple-element.12, bf16[768,896]{1,0:T(8,128)(2,1)S(1)} %copy-done.9), kind=kOutput, calls=%fused_computation.4 | convolution fusion | flops 2820407296 | bytes 8192000 | tf_op jit(solution)/shard_map/dot_general | solution.py:28
  136.2 0.0 copy-done.6
  136.2 0.0 copy-done.8
  136.2 4.9 %convert_bitcast_fusion.1 = bf16[1,2048,896]{2,1,0:T(8,128)(2,1)} fusion(bf16[768,2048]{1,0:T(8,128)(2,1)S(1)} %copy-done.6, bf16[768,896]{1,0:T(8,128)(2,1)S(1)} %copy-done.8), kind=kOutput, calls=%fused_computation.3 | convolution fusion | flops 2820407296 | bytes 8192000 | tf_op jit(solution)/shard_map/dot_general | solution.py:28
  141.1 0.0 copy-done.5
  141.1 0.0 copy-done.7
  141.1 4.5 %convert_bitcast_fusion = bf16[1,896,2048]{2,1,0:T(8,128)(2,1)} fusion(bf16[768,896]{1,0:T(8,128)(2,1)S(1)} %copy-done.7, bf16[768,2048]{1,0:T(8,128)(2,1)S(1)} %copy-done.5), kind=kOutput, calls=%fused_computation.2 | convolution fusion | flops 2820407296 | bytes 8192000 | tf_op jit(solution)/shard_map/dot_general | solution.py:28
  145.6 3.2 %fusion.87 = (f32[128]{0:T(128)S(1)}, f32[128]{0:T(128)S(1)}, f32[128,1024]{1,0:T(8,128)S(1)}) fusion(f32[128]{0:T(128)S(1)} %get-tuple-element.61, f32[128]{0:T(128)S(1)} %get-tuple-element.62, bf16[128,1024]{1,0:T(8,128)(2,1)S(1)} %copy-done, f32[1024]{0:T(1024)S(1)} %copy-done.4, bf16[128,2048]{0,1:T(8,128)(2,1)S(1)} %bitcast.87, ...), kind=kOutput, calls=%fused_computation.157 | convolution fusion | flops 538967808 | bytes 5511168 | tf_op jit(solution)/shard_map/dot_general | solution.py:24
  148.8 1.9 all-gather.7
  150.7 1.8 all-gather.6
  152.5 0.3 fusion.26
  152.8 1.3 collective-permute-start
  154.1 28.1 %all-to-all-done.1 = bf16[64,32,1024]{2,1,0:T(8,128)(2,1)} async-done(((bf16[64,32,1024]{2,1,0:T(8,128)(2,1)}), bf16[64,32,1024]{2,1,0:T(8,128)(2,1)}, u32[]{:S(2)}, u32[]{:S(2)}) %all-to-all-start.1) | async-done | bytes 4194336 | tf_op jit(solution)/shard_map/all_to_all | solution.py:371
  182.2 3.7 %convert_reduce_fusion = f32[32,1024]{1,0:T(8,128)} fusion(bf16[64,32,1024]{2,1,0:T(8,128)(2,1)} %all-to-all-done.1), kind=kLoop, calls=%fused_computation | loop fusion | flops 4161536 | bytes 4325376 | tf_op jit(solution)/shard_map/reduce_sum | solution.py:372
  185.9 0.0 collective-permute-done
  185.9 0.1 maximum_convert_fusion
  186.0 2.7 %fusion.28 = bf16[128,1024]{1,0:T(8,128)(2,1)} fusion(f32[158,1024]{1,0:T(8,128)S(1)} %maximum_convert_fusion, f32[1024]{0:T(1024)S(1)} %bitcast.103, f32[1024]{0:T(1024)S(1)} %bitcast.102, f32[1024]{0:T(1024)S(1)} %bitcast.101, f32[1024]{0:T(1024)S(1)} %bitcast.100, f32[1024]{0:T(1024)S(1)} %bitcast.99, f32[1024]{0:T(1024)S(1)} %bitcast.98, ...), kind=kLoop, calls=%fused_computation.47 | loop fusion | flops 8126464 | bytes 16642048 | tf_op jit(solution)/shard_map/convert_element_type | solution.py:445
  (17 shorter events, 0.3 us)
Async XLA Ops:
  7.2 9.6 %copy-start.1 = (bf16[128,1024]{1,0:T(8,128)(2,1)S(1)}, bf16[128,1024]{1,0:T(8,128)(2,1)}, u32[]{:S(2)}) copy-start(bf16[128,1024]{1,0:T(8,128)(2,1)} %param.16) | copy-start | bytes 786436
  7.2 9.3 %copy-start.2 = (bf16[128,1024]{1,0:T(8,128)(2,1)S(1)}, bf16[128,1024]{1,0:T(8,128)(2,1)}, u32[]{:S(2)}) copy-start(bf16[128,1024]{1,0:T(8,128)(2,1)} %param.15) | copy-start | bytes 786436
  7.2 138.4 %all-gather.10.cloned.1.call-start = ((), (), s32[]{:S(2)}) async-start(), calls=%async_computation.2 | async-start | bytes 4259840 | tf_op jit(solution)/shard_map/all_gather | solution.py:429
  107.3 5.8 %copy-start = (bf16[128,1024]{1,0:T(8,128)(2,1)S(1)}, bf16[128,1024]{1,0:T(8,128)(2,1)}, u32[]{:S(2)}) copy-start(bf16[128,1024]{1,0:T(8,128)(2,1)} %param.11) | copy-start | bytes 786436
  107.3 9.6 %copy-start.4 = (f32[1024]{0:T(1024)S(1)}, f32[1024]{0:T(1024)}, u32[]{:S(2)}) copy-start(f32[1024]{0:T(1024)} %param.12) | copy-start | bytes 12292
  108.8 8.1 %all-to-all-start = ((bf16[2,128,1024]{1,2,0:T(8,128)(2,1)}), bf16[2,128,1024]{1,2,0:T(8,128)(2,1)S(1)}, u32[]{:S(2)}, u32[]{:S(2)}) async-start(bf16[2,128,1024]{1,2,0:T(8,128)(2,1)} %broadcast_in_dim.8), calls=%async_computation | async-start | bytes 1048576 | tf_op jit(solution)/shard_map/all_to_all | solution.py:359
  120.3 8.4 %copy-start.3 = (bf16[31,1024]{1,0:T(8,128)(2,1)S(1)}, bf16[31,1024]{1,0:T(8,128)(2,1)}, u32[]{:S(2)}) copy-start(bf16[31,1024]{1,0:T(8,128)(2,1)} %param.13) | copy-start | bytes 190468
  120.3 8.5 %copy-start.9 = (bf16[768,896]{1,0:T(8,128)(2,1)S(1)}, bf16[768,896]{1,0:T(8,128)(2,1)}, u32[]{:S(2)}) copy-start(bf16[768,896]{1,0:T(8,128)(2,1)} %get-tuple-element.13) | copy-start | bytes 4128772
  120.3 61.9 %all-to-all-start.1 = ((bf16[64,32,1024]{2,1,0:T(8,128)(2,1)}), bf16[64,32,1024]{2,1,0:T(8,128)(2,1)}, u32[]{:S(2)}, u32[]{:S(2)}) async-start(bf16[64,32,1024]{2,1,0:T(8,128)(2,1)} %bitcast.85), calls=%async_computation.1 | async-start | bytes 8388608 | tf_op jit(solution)/shard_map/all_to_all | solution.py:371
  128.8 7.4 %copy-start.6 = (bf16[768,2048]{1,0:T(8,128)(2,1)S(1)}, bf16[768,2048]{1,0:T(8,128)(2,1)}, u32[]{:S(2)}) copy-start(bf16[768,2048]{1,0:T(8,128)(2,1)} %get-tuple-element.12) | copy-start | bytes 9437188
  128.8 7.4 %copy-start.8 = (bf16[768,896]{1,0:T(8,128)(2,1)S(1)}, bf16[768,896]{1,0:T(8,128)(2,1)}, u32[]{:S(2)}) copy-start(bf16[768,896]{1,0:T(8,128)(2,1)} %get-tuple-element.14) | copy-start | bytes 4128772
  136.2 4.9 %copy-start.5 = (bf16[768,2048]{1,0:T(8,128)(2,1)S(1)}, bf16[768,2048]{1,0:T(8,128)(2,1)}, u32[]{:S(2)}) copy-start(bf16[768,2048]{1,0:T(8,128)(2,1)} %get-tuple-element.16) | copy-start | bytes 9437188
  136.2 4.9 %copy-start.7 = (bf16[768,896]{1,0:T(8,128)(2,1)S(1)}, bf16[768,896]{1,0:T(8,128)(2,1)}, u32[]{:S(2)}) copy-start(bf16[768,896]{1,0:T(8,128)(2,1)} %get-tuple-element.15) | copy-start | bytes 4128772
  152.8 33.1 %collective-permute-start = (bf16[30,1024]{1,0:T(8,128)(2,1)S(1)}, bf16[30,1024]{1,0:T(8,128)(2,1)S(1)}, u32[]{:S(2)}, u32[]{:S(2)}) collective-permute-start(bf16[30,1024]{1,0:T(8,128)(2,1)S(1)} %slice.331), channel_id=1, source_target_pairs={{2,0},{4,2},{6,4},{8,6},{10,8},{12,10},{14,12},{16,14},{18,16},{20... | collective-permute-start | bytes 184328 | tf_op jit(solution)/shard_map/ppermute | solution.py:437
Sparse Core Ops, SparseCore 0:
  10.9 96.5 all-gather.9

commit v2 on v1

--- a/solution.py
+++ b/solution.py
@@ -47,13 +47,14 @@
 
 
 def expert_kernel(
-    pk, wg_hbm, wu_hbm, wd_hbm,
-    xs_out, ps_out, a_out, dg_out, du_out, ret_out,
+    pk, conv, gain, wg_hbm, wu_hbm, wd_hbm, proj_hbm,
+    xs_out, ps_out, a_out, dg_out, du_out, ret_out, proj_out, act_out, stats_out,
     wg, wu, wd, own, oth, xs, ps, acts, dgs, dus,
     psend, precv, pown, rsend, ret,
-    sel_a, sel_b,
+    sel_a, sel_b, proj, act, stat_send, stat_recv, stats,
     w_sem, a_send, b_send, c_send, own_sem, oth_sem,
     e_send, e_recv, r_send, r_recv, o_sem,
+    g_send, g_recv, s_send, s_recv, t_send, t_recv,
 ):
     me = lax.axis_index("sp")
     tp = lax.axis_index("tp")
@@ -64,6 +65,8 @@
         pltpu.make_async_copy(src, dst, w_sem.at[i])
         for i, (src, dst) in enumerate(((wg_hbm, wg), (wu_hbm, wu), (wd_hbm, wd)))
     ]
+    proj_load = pltpu.make_async_copy(proj_hbm, proj.at[mz, my, mx], w_sem.at[3])
+    proj_load.start()
     for copy in loads:
         copy.start()
 
@@ -84,6 +87,12 @@
     sel_a[...] = (col == spot).astype(F32).astype(BF16)
     sel_b[...] = (col == spot + 4).astype(F32).astype(BF16)
     own[pl.ds(me, 1)] = pk[pl.ds(me // 2, 1)]
+    values = conv[...].astype(F32)
+    lane = lax.broadcasted_iota(jnp.int32, (128, 128), 1)
+    total = jnp.sum(values, axis=1, keepdims=True)
+    squares = jnp.sum(values * values, axis=1, keepdims=True)
+    stat_send[...] = jnp.where(lane == 0, total, squares)
+    proj_load.wait()
 
     pl.semaphore_wait(barrier, 64)
 
@@ -99,6 +108,77 @@
         return 0
 
     lax.fori_loop(1, 32, start_direct, 0)
+    stat_copy = tp_copy(stat_send, stat_recv, s_send, s_recv, peer)
+    stat_copy.start()
+
+    def gather(group, axis, part):
+        def at(d):
+            z, y, x = mz, my, mx
+            if axis == 0:
+                z = lax.rem(mz + d, 4)
+            elif axis == 1:
+                y = lax.rem(my + d, 4)
+            else:
+                x = lax.rem(mx + d, 4)
+            return z, y, x
+
+        def copy(d, send):
+            z, y, x = at(0) if send else at(4 - d)
+            to_z, to_y, to_x = at(d)
+            block = proj.at[part(z, y, x)]
+            return sp_copy(
+                block, block, g_send.at[group, d - 1], g_recv.at[group, d - 1],
+                to_z * 16 + to_y * 4 + to_x,
+            )
+
+        def start():
+            for d in (1, 3, 2):
+                copy(d, True).start()
+
+        def take():
+            for d in (1, 3, 2):
+                copy(d, False).wait_recv()
+
+        def sent():
+            for d in (1, 3, 2):
+                copy(d, True).wait_send()
+
+        return start, take, sent
+
+    every = slice(None)
+    low, mid_cols, high = pl.ds(0, 256), pl.ds(256, 512), pl.ds(768, 256)
+    first_hop = (
+        gather(0, 2, lambda z, y, x: (z, y, x, every, pl.ds(0, 768))),
+        gather(1, 1, lambda z, y, x: (z, y, x, every, high)),
+    )
+    second_hop = (
+        gather(2, 1, lambda z, y, x: (z, y, every, every, low)),
+        gather(3, 0, lambda z, y, x: (z, y, every, every, mid_cols)),
+        gather(4, 0, lambda z, y, x: (z, every, x, every, high)),
+    )
+    third_hop = (
+        gather(5, 0, lambda z, y, x: (z, every, every, every, low)),
+        gather(6, 1, lambda z, y, x: (every, y, every, every, mid_cols)),
+        gather(7, 2, lambda z, y, x: (every, every, x, every, high)),
+    )
+    for start, _, _ in first_hop:
+        start()
+
+    stat_copy.wait_recv()
+    both = stat_send[...] + stat_recv[...]
+    row_mean = both[:, 0:1] / D
+    row_var = both[:, 1:2] / D - row_mean * row_mean
+    inv_std = lax.rsqrt(row_var + 1e-06)
+    stats[...] = jnp.where(lane == 0, row_mean, inv_std)
+    scaled_z = (values - row_mean) * inv_std * gain[...]
+    act[pl.ds(mz, 1)] = (scaled_z * jax.nn.sigmoid(scaled_z)).astype(BF16)[None]
+
+    def act_copy(d, send):
+        z = mz if send else lax.rem(mz + 4 - d, 4)
+        return sp_copy(
+            act.at[z], act.at[z], t_send.at[d - 1], t_recv.at[d - 1],
+            lax.rem(mz + d, 4) * 16 + lax.rem(me, 16),
+        )
 
     def source(k, j, near):
         dz, dy, side = gray(k), gray(j // 2), lax.rem(j, 2)
@@ -146,11 +226,14 @@
             e_send.at[z], e_recv.at[z], peer,
         )
 
+    def slot(s):
+        return lax.rem(s, 2) * 32 + s // 2
+
     def ret_copy(s):
-        return sp_copy(rsend.at[s], ret.at[me], r_send.at[s], r_recv.at[me], s)
+        return sp_copy(rsend.at[s], ret.at[slot(me)], r_send.at[s], r_recv.at[me], s)
 
     def ret_arrived(s):
-        return sp_copy(rsend.at[s], ret.at[s], r_send.at[s], r_recv.at[s], s)
+        return sp_copy(rsend.at[s], ret.at[slot(s)], r_send.at[s], r_recv.at[s], s)
 
     def plane(k):
         return lax.rem(mz - gray(k) + 4, 4)
@@ -222,6 +305,12 @@
 
     take_direct(0)
     take_direct(1)
+    for d in (1, 3, 2):
+        act_copy(d, True).start()
+    for _, take, _ in first_hop:
+        take()
+    for start, _, _ in second_hop:
+        start()
     take_twin(0)
     for copy in loads:
         copy.wait()
@@ -241,19 +330,36 @@
         def _():
             give_back(k - 1)
 
+        @pl.when(k == 1)
+        def _():
+            for _, take, _ in second_hop:
+                take()
+            for start, _, _ in third_hop:
+                start()
+
         return 0
 
     lax.fori_loop(0, 4, step, 0)
     outs = [
         pltpu.make_async_copy(src, dst, o_sem.at[i])
         for i, (src, dst) in enumerate(
-            ((xs, xs_out), (ps, ps_out), (acts, a_out), (dgs, dg_out), (dus, du_out))
+            ((xs, xs_out), (ps, ps_out), (acts, a_out), (dgs, dg_out), (dus, du_out), (stats, stats_out))
         )
     ]
     for copy in outs:
         copy.start()
     give_back(3)
-    ret[pl.ds(me, 1)] = rsend[pl.ds(me, 1)]
+    ret[pl.ds(slot(me), 1)] = rsend[pl.ds(me, 1)]
+    for _, take, _ in third_hop:
+        take()
+    for d in (1, 2, 3):
+        act_copy(d, False).wait_recv()
+    more = [
+        pltpu.make_async_copy(src, dst, o_sem.at[6 + i])
+        for i, (src, dst) in enumerate(((proj, proj_out), (act, act_out)))
+    ]
+    for copy in more:
+        copy.start()
 
     def finish_sends(i, _):
         @pl.when(i > 0)
@@ -278,14 +384,21 @@
     lax.fori_loop(0, 64, finish, 0)
     for z in range(4):
         part_copy(z).wait_send()
-    last = pltpu.make_async_copy(ret, ret_out, o_sem.at[5])
+    for _, _, sent in first_hop + second_hop + third_hop:
+        sent()
+    for d in (1, 2, 3):
+        act_copy(d, True).wait_send()
+    stat_copy.wait_send()
+    last = pltpu.make_async_copy(ret, ret_out, o_sem.at[8])
     last.start()
+    for copy in more:
+        copy.wait()
     for copy in outs:
         copy.wait()
     last.wait()
 
 
-def run_experts(pk, wg, wu, wd):
+def run_experts(pk, conv, gain, wg, wu, wd, proj):
     hidden = wg.shape[1]
     rows = 768
     out = [
@@ -295,13 +408,16 @@
         jax.ShapeDtypeStruct((rows, hidden), BF16),
         jax.ShapeDtypeStruct((rows, hidden), BF16),
         jax.ShapeDtypeStruct((64, 8, 1536), BF16),
+        jax.ShapeDtypeStruct((4, 4, 4, 32, HALF), BF16),
+        jax.ShapeDtypeStruct((4, 128, HALF), BF16),
+        jax.ShapeDtypeStruct((128, 128), F32),
     ]
     dma = pltpu.SemaphoreType.DMA
     return pl.pallas_call(
         expert_kernel,
         out_shape=out,
-        in_specs=[pl.BlockSpec(memory_space=pltpu.VMEM)] + [pl.BlockSpec(memory_space=pl.ANY)] * 3,
-        out_specs=[pl.BlockSpec(memory_space=pl.ANY)] * 6,
+        in_specs=[pl.BlockSpec(memory_space=pltpu.VMEM)] * 3 + [pl.BlockSpec(memory_space=pl.ANY)] * 4,
+        out_specs=[pl.BlockSpec(memory_space=pl.ANY)] * 9,
         scratch_shapes=[
             pltpu.VMEM((D, hidden), BF16),
             pltpu.VMEM((D, hidden), BF16),
@@ -320,14 +436,235 @@
             pltpu.VMEM((64, 8, 1536), BF16),
             pltpu.VMEM((64, 128), BF16),
             pltpu.VMEM((64, 128), BF16),
-            dma((3,)), dma((32,)), dma((32,)), dma((64,)), dma((64,)), dma((64,)),
-            dma((4,)), dma((4,)), dma((64,)), dma((64,)), dma((6,)),
+            pltpu.VMEM((4, 4, 4, 32, HALF), BF16),
+            pltpu.VMEM((4, 128, HALF), BF16),
+            pltpu.VMEM((128, 128), F32),
+            pltpu.VMEM((128, 128), F32),
+            pltpu.VMEM((128, 128), F32),
+            dma((4,)), dma((32,)), dma((32,)), dma((64,)), dma((64,)), dma((64,)),
+            dma((4,)), dma((4,)), dma((64,)), dma((64,)), dma((9,)),
+            dma((8, 3)), dma((8, 3)), dma, dma, dma((3,)), dma((3,)),
         ],
         compiler_params=pltpu.CompilerParams(
             collective_id=0, has_side_effects=True, vmem_limit_bytes=56 * 1024 * 1024
         ),
         name="experts",
-    )(pk, wg, wu, wd)
+    )(pk, conv, gain, wg, wu, wd, proj)
+
+
+def tail_kernel(
+    s_main, s_first, s_second, out_grad, conv, gain, taps, stats_in, ret_hbm, proj_hbm, act_hbm,
+    gin_out, gproj_out,
+    ret, proj, act, gs, gz, part, parts, ext, sum_send, sum_recv, taps_f,
+    l_sem, c_send, c_recv, z_send, z_recv, p_send, p_recv, u_send, u_recv, h_send, h_recv,
+):
+    me = lax.axis_index("sp")
+    tp = lax.axis_index("tp")
+    peer = 1 - tp
+    mz, here = me // 16, lax.rem(me, 16)
+    loads = [
+        pltpu.make_async_copy(src, dst, l_sem.at[i])
+        for i, (src, dst) in enumerate(((ret_hbm, ret), (proj_hbm, proj), (act_hbm, act)))
+    ]
+    for copy in loads:
+        copy.start()
+    barrier = pltpu.get_barrier_semaphore()
+
+    def greet(to):
+        pl.semaphore_signal(barrier, inc=1, device_id={"sp": to}, device_id_type=MESH)
+
+    def plane_peer(d):
+        return lax.rem(mz + d, 4) * 16 + here
+
+    def greet_plane(d, _):
+        greet(mz * 16 + lax.rem(here + d, 16))
+        return 0
+
+    lax.fori_loop(1, 16, greet_plane, 0)
+    for d in (1, 2, 3):
+        for core in (0, 1):
+            pl.semaphore_signal(
+                barrier, inc=1, device_id={"sp": plane_peer(d), "tp": core}, device_id_type=MESH
+            )
+    greet(lax.rem(me + 1, 64))
+    greet(lax.rem(me + 63, 64))
+    pl.semaphore_signal(barrier, inc=1, device_id={"tp": peer}, device_id_type=MESH)
+
+    loads[0].wait()
+    contrib = jnp.zeros((128, HALF), F32)
+    halves = []
+    for h in range(2):
+        block = ret[pl.ds(h * 32, 32)].reshape(256, 1536)
+        contrib = contrib + nn(s_main[...], block[:, :HALF])
+        halves.append(block[:, HALF:])
+    left = nn(s_first[...], halves[0]) + nn(s_first[...], halves[1])
+    right = nn(s_second[...], halves[0]) + nn(s_second[...], halves[1])
+    left = (out_grad[:, :512].astype(F32) + (contrib[:, :512] + left)).astype(BF16)
+    right = (out_grad[:, 512:].astype(F32) + (contrib[:, 512:] + right)).astype(BF16)
+    gs[pl.ds(2 * tp, 1)] = left[None]
+    gs[pl.ds(2 * tp + 1, 1)] = right[None]
+    pl.semaphore_wait(barrier, 24)
+
+    def core_copy(tp_of):
+        rows = pl.ds(2 * tp_of, 2)
+        return tp_copy(gs.at[rows], gs.at[rows], c_send, c_recv, peer)
+
+    def plane_copy(z, core, i):
+        return pltpu.make_async_remote_copy(
+            src_ref=gs.at[z], dst_ref=gz.at[mz],
+            send_sem=z_send.at[i, core], recv_sem=z_recv.at[mz],
+            device_id={"sp": z * 16 + here, "tp": core}, device_id_type=MESH,
+        )
+
+    def plane_arrived(z):
+        return sp_copy(gz.at[z], gz.at[z], z_send.at[0, 0], z_recv.at[z], z * 16 + here)
+
+    core_copy(tp).start()
+    for i in range(2):
+        z = 2 * tp + i
+
+        @pl.when(z != mz)
+        def _():
+            plane_copy(z, 0, i).start()
+            plane_copy(z, 1, i).start()
+
+    loads[1].wait()
+    loads[2].wait()
+
+    def weights(z):
+        return proj[pl.ds(z, 1)].reshape(512, HALF)
+
+    grad_act = nn(left, weights(2 * tp)) + nn(right, weights(2 * tp + 1))
+    core_copy(peer).wait_recv()
+    mine = gs[pl.ds(mz, 1)].reshape(128, 512)
+    total = tn(mine, act[pl.ds(mz, 1)].reshape(128, HALF))
+    for d in (1, 3, 2):
+        z = lax.rem(mz + d, 4)
+        plane_arrived(z).wait_recv()
+        total = total + tn(gz[pl.ds(z, 1)].reshape(128, 512), act[pl.ds(z, 1)].reshape(128, HALF))
+    part[...] = total.astype(BF16).reshape(16, 32, HALF)
+
+    def part_copy(d):
+        q = lax.rem(here + d, 16)
+        return sp_copy(part.at[q], parts.at[here], p_send.at[d], p_recv.at[here], mz * 16 + q)
+
+    def part_arrived(q):
+        return sp_copy(parts.at[q], parts.at[q], p_send.at[0], p_recv.at[q], mz * 16 + q)
+
+    def start_part(d, _):
+        part_copy(d).start()
+        return 0
+
+    other = gs[pl.ds(2 * peer, 2)]
+    grad_act = grad_act + nn(other[0], weights(2 * peer)) + nn(other[1], weights(2 * peer + 1))
+    lax.fori_loop(1, 16, start_part, 0)
+
+    row_mean, inv_std = stats_in[:, 0:1], stats_in[:, 1:2]
+    normed = (conv[...].astype(F32) - row_mean) * inv_std
+    scaled_z = normed * gain[...]
+    z_sig = jax.nn.sigmoid(scaled_z)
+    grad_normed = grad_act * z_sig * (1.0 + scaled_z * (1.0 - z_sig)) * gain[...]
+    lane = lax.broadcasted_iota(jnp.int32, (128, 128), 1)
+    sum_send[...] = jnp.where(
+        lane == 0,
+        jnp.sum(grad_normed, axis=1, keepdims=True),
+        jnp.sum(grad_normed * normed, axis=1, keepdims=True),
+    )
+    taps_f[pl.ds(0, 31), :] = taps[...].astype(F32)
+    sum_copy = tp_copy(sum_send, sum_recv, u_send, u_recv, peer)
+    sum_copy.start()
+    sum_copy.wait_recv()
+    both = sum_send[...] + sum_recv[...]
+    grad_conv = inv_std * (grad_normed - both[:, 0:1] / D - normed * (both[:, 1:2] / D))
+    ext[pl.ds(0, 128), :] = grad_conv.astype(BF16).astype(F32)
+
+    def reach_copy(to):
+        return sp_copy(ext.at[pl.ds(0, 32)], ext.at[pl.ds(128, 32)], h_send, h_recv, to)
+
+    @pl.when(me == 63)
+    def _():
+        ext[pl.ds(128, 32), :] = jnp.zeros((32, HALF), F32)
+
+    @pl.when(me > 0)
+    def _():
+        reach_copy(me - 1).start()
+
+    parts[pl.ds(here, 1)] = part[pl.ds(here, 1)]
+
+    @pl.when(me < 63)
+    def _():
+        reach_copy(me + 1).wait_recv()
+
+    def columns(c, _):
+        cols = pl.ds(pl.multiple_of(c * 128, 128), 128)
+        acc = jnp.zeros((128, 128), F32)
+        for k in range(31):
+            acc = acc + taps_f[pl.ds(k, 1), cols] * ext[pl.ds(k, 128), cols]
+        gin_out[:, cols] = acc.astype(BF16)
+        return 0
+
+    lax.fori_loop(0, 8, columns, 0)
+
+    def wait_part(d, _):
+        part_arrived(lax.rem(here + d, 16)).wait_recv()
+        return 0
+
+    lax.fori_loop(1, 16, wait_part, 0)
+    result = parts[0].astype(F32)
+    for q in range(1, 16):
+        result = result + parts[q].astype(F32)
+    gproj_out[...] = result
+
+    def sent_part(d, _):
+        part_copy(d).wait_send()
+        return 0
+
+    lax.fori_loop(1, 16, sent_part, 0)
+    core_copy(tp).wait_send()
+    sum_copy.wait_send()
+    for i in range(2):
+        z = 2 * tp + i
+
+        @pl.when(z != mz)
+        def _():
+            plane_copy(z, 0, i).wait_send()
+            plane_copy(z, 1, i).wait_send()
+
+    @pl.when(me > 0)
+    def _():
+        reach_copy(me - 1).wait_send()
+
+
+def run_tail(s_main, s_first, s_second, out_grad, conv, gain, taps, stats, ret, proj, act):
+    dma = pltpu.SemaphoreType.DMA
+    return pl.pallas_call(
+        tail_kernel,
+        out_shape=[
+            jax.ShapeDtypeStruct((128, HALF), BF16),
+            jax.ShapeDtypeStruct((32, HALF), F32),
+        ],
+        in_specs=[pl.BlockSpec(memory_space=pltpu.VMEM)] * 8 + [pl.BlockSpec(memory_space=pl.ANY)] * 3,
+        out_specs=[pl.BlockSpec(memory_space=pltpu.VMEM)] * 2,
+        scratch_shapes=[
+            pltpu.VMEM((64, 8, 1536), BF16),
+            pltpu.VMEM((4, 4, 4, 32, HALF), BF16),
+            pltpu.VMEM((4, 128, HALF), BF16),
+            pltpu.VMEM((4, 128, 512), BF16),
+            pltpu.VMEM((4, 128, 512), BF16),
+            pltpu.VMEM((16, 32, HALF), BF16),
+            pltpu.VMEM((16, 32, HALF), BF16),
+            pltpu.VMEM((160, HALF), F32),
+            pltpu.VMEM((128, 128), F32),
+            pltpu.VMEM((128, 128), F32),
+            pltpu.VMEM((32, HALF), F32),
+            dma((3,)), dma, dma, dma((2, 2)), dma((4,)), dma((16,)), dma((16,)),
+            dma, dma, dma, dma,
+        ],
+        compiler_params=pltpu.CompilerParams(
+            collective_id=1, has_side_effects=True, vmem_limit_bytes=40 * 1024 * 1024
+        ),
+        name="tail",
+    )(s_main, s_first, s_second, out_grad, conv, gain, taps, stats, ret, proj, act)
 
 
 def slots_of(route_block, experts):
@@ -350,33 +687,10 @@
     return main, first, second
 
 
-def total_of_pieces(array, axis):
-    return lax.all_gather(array, axis).sum(0)
-
-
-def gather_directly(array, axis, dim):
-    peers = lax.axis_size(axis)
-    blocks = lax.all_to_all(
-        jnp.broadcast_to(array[None], (peers, *array.shape)), axis, 0, 0, tiled=True
-    )
-    shape = list(array.shape)
-    shape[dim] *= peers
-    return jnp.moveaxis(blocks, 0, dim).reshape(shape)
-
-
-def summed_on_arrival(array, axis, dim):
-    peers = lax.axis_size(axis)
-    before, after = array.shape[:dim], array.shape[dim + 1 :]
-    blocks = jnp.moveaxis(array.reshape(*before, peers, -1, *after), dim, 0)
-    arrived = lax.all_to_all(blocks, axis, split_axis=0, concat_axis=0, tiled=True)
-    return arrived.astype(F32).sum(axis=0)
-
-
 def on_device(
     conv_out, ln_gain, taps, proj_weight, stream_mid, out_grad,
     routes, route_probs, gate_slabs, up_slabs, down_slabs,
 ):
-    tok_rows = conv_out.shape[0]
     experts = lax.axis_size("sp") // 2
     main, first, second = tables(routes, experts)
 
@@ -400,49 +714,18 @@
         axis=1,
     ).reshape(experts, MAIN, 3072)
 
-    xs, ps, acts, dg, du, ret = run_experts(pk, gate_slabs[0], up_slabs[0], down_slabs[0])
+    gain = ln_gain[None, :]
+    xs, ps, acts, dg, du, ret, proj, act, stats = run_experts(
+        pk, conv_out, gain, gate_slabs[0], up_slabs[0], down_slabs[0], proj_weight
+    )
+    grad_input, grad_proj = run_tail(
+        s_main, s_first, s_second, out_grad, conv_out, gain, taps, stats, ret, proj, act
+    )
     grad_down = tn(acts, ps).astype(BF16)
     grad_gate = tn(xs, dg).astype(BF16)
     grad_up = tn(xs, du).astype(BF16)
-
-    pairs = ret.reshape(experts, 2, MAIN, 1536)
-    contrib = 0.0
-    for h in range(2):
-        rows = pairs[:, h].reshape(experts * MAIN, 1536)
-        contrib = contrib + nn(s_main, rows[:, :HALF])
-        contrib = contrib + jnp.concatenate(
-            [nn(s_first, rows[:, HALF:]), nn(s_second, rows[:, HALF:])], axis=1
-        )
-    grad_stream = (out_grad.astype(F32) + contrib).astype(BF16)
-
-    values = conv_out.astype(F32)
-    row_total = total_of_pieces(jnp.sum(values, axis=1), "tp")
-    row_squares = total_of_pieces(jnp.sum(values * values, axis=1), "tp")
-    row_mean = row_total[:, None] / D
-    row_var = row_squares[:, None] / D - row_mean * row_mean
-    inv_std = lax.rsqrt(row_var + 1e-06)
-    normed = (values - row_mean) * inv_std
-    scaled_z = normed * ln_gain[None, :]
-    z_sig = jax.nn.sigmoid(scaled_z)
-    activated = (scaled_z * z_sig).astype(BF16)
-    whole_stream = gather_directly(grad_stream, "tp", 1)
-    grad_act = nn(whole_stream, lax.all_gather(proj_weight, "sp", axis=0, tiled=True))
-    grad_normed = grad_act * z_sig * (1.0 + scaled_z * (1.0 - z_sig)) * ln_gain[None, :]
-    first_sum = total_of_pieces(jnp.sum(grad_normed, axis=1), "tp")
-    second_sum = total_of_pieces(jnp.sum(grad_normed * normed, axis=1), "tp")
-    grad_conv = (
-        inv_std * (grad_normed - first_sum[:, None] / D - normed * second_sum[:, None] / D)
-    ).astype(BF16)
-    reach = taps.shape[0] - 1
-    following = lax.ppermute(grad_conv[:reach], "sp", [(k, k - 1) for k in range(1, 64)])
-    extended = jnp.concatenate([grad_conv, following], axis=0).astype(F32)
-    tap_values = taps.astype(F32)
-    grad_input = jnp.zeros((tok_rows, grad_conv.shape[1]), F32)
-    for offset in range(taps.shape[0]):
-        grad_input = grad_input + tap_values[offset][None, :] * extended[offset : offset + tok_rows]
-    grad_proj = summed_on_arrival(tn(whole_stream, activated).astype(BF16), "sp", 0)
     return (
-        grad_input.astype(BF16), grad_proj, grad_gate[None], grad_up[None], grad_down[None],
+        grad_input, grad_proj, grad_gate[None], grad_up[None], grad_down[None],
     )
 
 

time: 197 us -> 166 us (0.84)
  Pallas kernels: 86.7 us -> 132 us
  waiting for transfers between devices: 28.8 us -> 0 us
  starting transfers between devices: 13.9 us -> 0 us
  between operations: 14.3 us -> 0.81 us
  matrix products: 30.1 us -> 20.1 us
  blocking collectives: 7.31 us -> 0 us
  other arithmetic: 11.7 us -> 4.77 us
  local copies, waits for them, and re-layouts: 2.63 us -> 7.04 us
    pallas_call x0 -> x1, Pallas kernels: none -> 30.6 us  [run_tail(): pl.pallas_call(tail_kernel, out_shape=[jax.ShapeDtypeStruct((128, HALF),...]
    all_to_all x2 -> x0, waiting for transfers between devices: 28.1 us -> none  [the longest x1 28.1 us: summed_on_arrival(): lax.all_to_all(blocks, axis, split_axis=0, concat_axis=0, tiled=True)]
    pallas_call x1, Pallas kernels: 86.7 us -> 102 us  [run_experts(): pl.pallas_call(expert_kernel, out_shape=out, in_specs=[pl.BlockSpec(memor...]
    all_to_all x2 -> x0, starting transfers between devices: 12.6 us -> none  [the longest x1 8.34 us: summed_on_arrival(): lax.all_to_all(blocks, axis, split_axis=0, concat_axis=0, tiled=True)]
    all_gather x4 -> x0, blocking collectives: 7.31 us -> none  [total_of_pieces(): return lax.all_gather(array, axis).sum(0)]
    unnamed x20 -> x28, local copies, waits for them, and re-layouts: 0.05 us -> 7.04 us
    dot_general x10 -> x9, matrix products: 25.6 us -> 20 us  [tn(): lax.dot_general(a, b, (((0,), (0,)), ((), ())), preferred_element_type=F32)]
    dot_general x7 -> x0, matrix products: 4.4 us -> none  [nn(): lax.dot_general(a, b, (((1,), (0,)), ((), ())), preferred_element_type=F32)]
  transfers between devices with their start and end apart: 4 -> 0, of which waited for: 1 -> 0; matrix products, arithmetic and copies ran while one was open for 21% -> 0% of each run, Pallas kernels for 44% -> 0%
where the time goes in v2:
time: 166 us; the launch traced here: 165 us
  Pallas kernels  132 us (80%)
  matrix products  20.1 us (12%)
  local copies, waits for them, and re-layouts  7.04 us (4%)
  other arithmetic  4.77 us (3%)
    pallas_call x1, Pallas kernels, run_experts(): pl.pallas_call(expert_kernel, out_shape=out, in_specs=[pl.BlockSpec(memor...  102 us
    pallas_call x1, Pallas kernels, run_tail(): pl.pallas_call(tail_kernel, out_shape=[jax.ShapeDtypeStruct((128, HALF),...  30.6 us
    dot_general x9, matrix products, tn(): lax.dot_general(a, b, (((0,), (0,)), ((), ())), preferred_element_type=F32)  20 us
    unnamed x28, local copies, waits for them, and re-layouts  7.04 us

profile of v2, /device:TPU:1, one launch (start us, length us, event | category | flops | bytes accessed | tf_op | source)
XLA Modules:
  0.0 165.0 jit_solution(9779957075109415848)
XLA Ops:
  0.6 0.0 copy-start.1
  0.6 0.7 convert_reduce_fusion
  1.4 0.1 fusion.16
  1.5 0.7 select_reduce_fusion.3
  2.2 0.7 broadcast_add_fusion
  2.9 1.0 select_reduce_fusion
  3.9 0.2 fusion.6
  4.3 1.3 fusion
  5.6 1.3 convolution_convert_fusion
  6.9 1.2 fusion.11
  8.1 1.2 fusion.3
  9.3 0.0 copy-done.1
  9.4 0.3 fusion.8
  9.6 0.3 fusion.2
  9.9 1.3 maximum_bitcast_fusion.pk
  11.2 0.0 copy-start.4
  11.2 0.0 copy-start.5
  11.2 0.0 copy-start.7
  11.2 101.7 %experts.1 = (bf16[768,2048]{1,0:T(8,128)(2,1)}, bf16[768,2048]{1,0:T(8,128)(2,1)}, bf16[768,896]{1,0:T(8,128)(2,1)}, bf16[768,896]{1,0:T(8,128)(2,1)}, bf16[768...) custom-call(bf16[32,8,3072]{2,1,0:T(8,128)(2,1)} %maximum_bitcast_fu, ...), custom_call_target="tpu_custom_call" | custom-call | tf_op jit(solution)/shard_map/experts/pallas_call | solution.py:416
  112.9 0.0 copy-done.4
  112.9 0.0 copy-done.5
  112.9 0.0 copy-done.7
  112.9 0.0 copy-start
  112.9 2.2 %copy-done = bf16[4,4,4,32,1024]{4,3,2,1,0:T(8,128)(2,1)S(1)} copy-done((bf16[4,4,4,32,1024]{4,3,2,1,0:T(8,128)(2,1)S(1)}, bf16[4,4,4,32,1024]{4,3,2,1,0:T(8,128)(2,1)}, u32[]{:S(2)}) %copy-start) | copy-done | bytes 4194328
  115.1 0.0 copy-start.2
  115.1 1.4 copy-done.2
  116.5 0.0 copy-start.3
  116.5 1.2 copy-done.3
  117.8 0.0 copy-start.6
  117.8 0.8 copy-done.6
  118.6 0.0 copy-start.9
  118.6 0.0 copy-start.12
  118.6 30.6 %tail.1 = (bf16[128,1024]{1,0:T(8,128)(2,1)S(1)}, f32[32,1024]{1,0:T(8,128)S(1)}) custom-call(bf16[128,256]{1,0:T(8,128)(2,1)S(1)} %fusion.19.s_main, bf16[128,256]{1,0:T(8,128)(2,1)S(1)} %fusion.22.s_first, bf16[128,256]{1,0:T(8,128)(2,1)S(1)} %fusion.25.s_second, bf16[128,1024]{1,0:T(8,128)(2,1)S(1)} %copy-done.1, bf16[128,1024]{1,0:T(8,128)(2,1)S(1)} %copy-done.4, ...), custom_call_target="tpu_custom_call" | custom-call | tf_op jit(solution)/shard_map/tail/pallas_call | solution.py:640
  149.2 0.0 copy-done.9
  149.2 0.0 copy-done.12
  149.2 0.0 copy-start.11
  149.2 5.0 %convert_bitcast_fusion.2 = bf16[1,2048,896]{2,1,0:T(8,128)(2,1)} fusion(bf16[768,2048]{1,0:T(8,128)(2,1)S(1)} %copy-done.9, bf16[768,896]{1,0:T(8,128)(2,1)S(1)} %copy-done.12), kind=kOutput, calls=%fused_computation.2 | convolution fusion | flops 2820407296 | bytes 8192000 | tf_op jit(solution)/shard_map/dot_general | solution.py:28
  154.2 0.0 copy-done.11
  154.2 0.0 copy-start.8
  154.2 0.0 copy-start.10
  154.2 5.0 %convert_bitcast_fusion.1 = bf16[1,2048,896]{2,1,0:T(8,128)(2,1)} fusion(bf16[768,2048]{1,0:T(8,128)(2,1)S(1)} %copy-done.9, bf16[768,896]{1,0:T(8,128)(2,1)S(1)} %copy-done.11), kind=kOutput, calls=%fused_computation.1 | convolution fusion | flops 2820407296 | bytes 8192000 | tf_op jit(solution)/shard_map/dot_general | solution.py:28
  159.2 0.0 copy-done.8
  159.2 0.0 copy-done.10
  159.2 4.5 %convert_bitcast_fusion = bf16[1,896,2048]{2,1,0:T(8,128)(2,1)} fusion(bf16[768,896]{1,0:T(8,128)(2,1)S(1)} %copy-done.10, bf16[768,2048]{1,0:T(8,128)(2,1)S(1)} %copy-done.8), kind=kOutput, calls=%fused_computation | convolution fusion | flops 2820407296 | bytes 8192000 | tf_op jit(solution)/shard_map/dot_general | solution.py:28
  163.7 0.7 copy.23
  164.4 0.7 copy.24
  (6 shorter events, 0.2 us)
Async XLA Ops:
  0.6 8.7 %copy-start.1 = (bf16[128,1024]{1,0:T(8,128)(2,1)S(1)}, bf16[128,1024]{1,0:T(8,128)(2,1)}, u32[]{:S(2)}) copy-start(bf16[128,1024]{1,0:T(8,128)(2,1)} %out_grad.1) | copy-start | bytes 786436
  11.2 101.7 %copy-start.4 = (bf16[128,1024]{1,0:T(8,128)(2,1)S(1)}, bf16[128,1024]{1,0:T(8,128)(2,1)}, u32[]{:S(2)}) copy-start(bf16[128,1024]{1,0:T(8,128)(2,1)} %conv.3) | copy-start | bytes 786436
  11.2 101.7 %copy-start.5 = (bf16[31,1024]{1,0:T(8,128)(2,1)S(1)}, bf16[31,1024]{1,0:T(8,128)(2,1)}, u32[]{:S(2)}) copy-start(bf16[31,1024]{1,0:T(8,128)(2,1)} %taps.1) | copy-start | bytes 190468
  11.2 101.7 %copy-start.7 = (f32[1024]{0:T(1024)S(1)}, f32[1024]{0:T(1024)}, u32[]{:S(2)}) copy-start(f32[1024]{0:T(1024)} %param.12) | copy-start | bytes 12292
  112.9 2.2 %copy-start = (bf16[4,4,4,32,1024]{4,3,2,1,0:T(8,128)(2,1)S(1)}, bf16[4,4,4,32,1024]{4,3,2,1,0:T(8,128)(2,1)}, u32[]{:S(2)}) copy-start(bf16[4,4,4,32,1024]{4,3,2,1,0:T(8,128)(2,1)} %get-tuple-element.18.proj_hbm) | copy-start | bytes 12582916
  115.1 1.4 copy-start.2
  116.5 1.2 copy-start.3
  117.8 0.8 copy-start.6
  118.6 30.6 %copy-start.9 = (bf16[768,2048]{1,0:T(8,128)(2,1)S(1)}, bf16[768,2048]{1,0:T(8,128)(2,1)}, u32[]{:S(2)}) copy-start(bf16[768,2048]{1,0:T(8,128)(2,1)} %get-tuple-element.22) | copy-start | bytes 9437188
  118.6 30.6 %copy-start.12 = (bf16[768,896]{1,0:T(8,128)(2,1)S(1)}, bf16[768,896]{1,0:T(8,128)(2,1)}, u32[]{:S(2)}) copy-start(bf16[768,896]{1,0:T(8,128)(2,1)} %get-tuple-element.23) | copy-start | bytes 4128772
  149.2 5.0 %copy-start.11 = (bf16[768,896]{1,0:T(8,128)(2,1)S(1)}, bf16[768,896]{1,0:T(8,128)(2,1)}, u32[]{:S(2)}) copy-start(bf16[768,896]{1,0:T(8,128)(2,1)} %get-tuple-element.24) | copy-start | bytes 4128772
  154.2 5.0 %copy-start.8 = (bf16[768,2048]{1,0:T(8,128)(2,1)S(1)}, bf16[768,2048]{1,0:T(8,128)(2,1)}, u32[]{:S(2)}) copy-start(bf16[768,2048]{1,0:T(8,128)(2,1)} %get-tuple-element.26) | copy-start | bytes 9437188
  154.2 5.0 %copy-start.10 = (bf16[768,896]{1,0:T(8,128)(2,1)S(1)}, bf16[768,896]{1,0:T(8,128)(2,1)}, u32[]{:S(2)}) copy-start(bf16[768,896]{1,0:T(8,128)(2,1)} %get-tuple-element.25) | copy-start | bytes 4128772

commit v3 on v2

v3 whole, which is shorter than its diff:
```python
import functools

import jax
import jax.numpy as jnp
from jax import lax
from jax.experimental import pallas as pl
from jax.experimental.pallas import tpu as pltpu
from jax.sharding import PartitionSpec as P

D = 2048
HALF = 1024
MAIN = 8
REM = 4
MESH = pl.DeviceIdType.MESH
F32 = jnp.float32
BF16 = jnp.bfloat16
VMEM_BYTES = 42 * 1024 * 1024


def nt(a, b):
    return lax.dot_general(a, b, (((1,), (1,)), ((), ())), preferred_element_type=F32)


def nn(a, b):
    return lax.dot_general(a, b, (((1,), (0,)), ((), ())), preferred_element_type=F32)


def tn(a, b):
    return lax.dot_general(a, b, (((0,), (0,)), ((), ())), preferred_element_type=F32)


def sp_copy(src, dst, send, recv, sp):
    return pltpu.make_async_remote_copy(
        src_ref=src, dst_ref=dst, send_sem=send, recv_sem=recv,
        device_id={"sp": sp}, device_id_type=MESH,
    )


def tp_copy(src, dst, send, recv, tp):
    return pltpu.make_async_remote_copy(
        src_ref=src, dst_ref=dst, send_sem=send, recv_sem=recv,
        device_id={"tp": tp}, device_id_type=MESH,
    )


def gray(k):
    return lax.rem(k + k // 2 - 2 * (k // 3), 4)


def layer_kernel(
    routes, probs, stream, out_grad, conv, gain, taps, wg_hbm, wu_hbm, wd_hbm, proj_hbm,
    gin_out, gproj_out, wg, wu, wd,
    pk, own, oth, xs, ps, acts, dgs, dus, psend, precv, pown, ret,
    table, sel_a, sel_b, proj, act, stat_send, stat_recv, stats,
    gs, gz, part, parts, ext, sum_send, sum_recv, taps_f,
    w_sem, a_send, b_send, c_send, own_sem, oth_sem,
    e_send, e_recv, r_send, r_recv,
    g_send, g_recv, s_send, s_recv, t_send, t_recv,
    q_send, q_recv, z_send, z_recv, p_send, p_recv, u_send, u_recv, h_send, h_recv,
):
    me = lax.axis_index("sp")
    tp = lax.axis_index("tp")
    peer = 1 - tp
    mx, my, mz = lax.rem(me, 4), lax.rem(me // 4, 4), me // 16
    here = lax.rem(me, 16)
    twin = me + 1 - 2 * lax.rem(me, 2)
    loads = [
        pltpu.make_async_copy(src, dst, w_sem.at[i])
        for i, (src, dst) in enumerate(((wg_hbm, wg), (wu_hbm, wu), (wd_hbm, wd)))
    ]
    proj_load = pltpu.make_async_copy(proj_hbm, proj.at[mz, my, mx], w_sem.at[3])
    proj_load.start()
    for copy in loads:
        copy.start()

    barrier = pltpu.get_barrier_semaphore()

    def greet(k, _):
        pl.semaphore_signal(
            barrier, inc=1, device_id={"sp": lax.rem(me + k, 64)}, device_id_type=MESH
        )
        return 0

    lax.fori_loop(1, 64, greet, 0)
    pl.semaphore_signal(barrier, inc=1, device_id={"tp": peer}, device_id_type=MESH)
    for d in (1, 2, 3):
        pl.semaphore_signal(
            barrier, inc=1, device_id={"sp": lax.rem(mz + d, 4) * 16 + here, "tp": peer},
            device_id_type=MESH,
        )

    expert = lax.broadcasted_iota(jnp.int32, (128, 128), 0)
    other = lax.broadcasted_iota(jnp.int32, (128, 128), 1)
    picks = [expert == routes[j : j + 1, :] for j in range(2)]
    counts = picks[0].astype(F32) + picks[1].astype(F32)
    before = nn(counts.astype(BF16), (expert < other).astype(F32).astype(BF16))
    at = lax.broadcasted_iota(jnp.int32, (256, 128), 0)
    for j in range(2):
        slot_row = jnp.sum(jnp.where(picks[j], before, 0.0), axis=0, keepdims=True)
        slot_row = slot_row.astype(jnp.int32)
        base = routes[j : j + 1, :] * MAIN + slot_row
        near = jnp.where(slot_row < MAIN, base, -1)
        far = jnp.where(slot_row < MAIN, -1, base)
        table[3 * j] = (at == near).astype(F32).astype(BF16)
        table[3 * j + 1] = (at + MAIN == far).astype(F32).astype(BF16)
        table[3 * j + 2] = (at + REM == far).astype(F32).astype(BF16)
    for i in range(3):
        table[6 + i] = table[i] + table[3 + i]
    shape = (32, 8, HALF)
    pk[:, :, :HALF] = nn(table[6], stream[...]).astype(BF16).reshape(shape)
    rest = nn(table[7], stream[:, :512]) + nn(table[8], stream[:, 512:])
    pk[:, :, 2 * HALF : 2 * HALF + 512] = rest.astype(BF16).reshape(32, 8, 512)
    grads = []
    for j in range(2):
        prob = jnp.broadcast_to(probs[j : j + 1, :], (128, 128)).T[:, 0:1]
        grads.append((out_grad[...].astype(F32) * prob).astype(BF16))
    near = nn(table[0], grads[0]) + nn(table[3], grads[1])
    pk[:, :, HALF : 2 * HALF] = near.astype(BF16).reshape(shape)
    rest = nn(table[1], grads[0][:, :512]) + nn(table[4], grads[1][:, :512])
    rest = rest + nn(table[2], grads[0][:, 512:]) + nn(table[5], grads[1][:, 512:])
    pk[:, :, 2 * HALF + 512 :] = rest.astype(BF16).reshape(32, 8, 512)

    row = lax.broadcasted_iota(jnp.int32, (64, 128), 0)
    col = lax.broadcasted_iota(jnp.int32, (64, 128), 1)
    spot = (row // 4) * 8 + row % 4
    sel_a[...] = (col == spot).astype(F32).astype(BF16)
    sel_b[...] = (col == spot + 4).astype(F32).astype(BF16)
    own[pl.ds(me, 1)] = pk[pl.ds(me // 2, 1)]
    values = conv[...].astype(F32)
    lane = lax.broadcasted_iota(jnp.int32, (128, 128), 1)
    total = jnp.sum(values, axis=1, keepdims=True)
    squares = jnp.sum(values * values, axis=1, keepdims=True)
    stat_send[...] = jnp.where(lane == 0, total, squares)
    proj_load.wait()

    pl.semaphore_wait(barrier, 67)

    def direct_send(i):
        k, j = i // 8, lax.rem(i, 8)
        dz, dy, side = gray(k), gray(j // 2), lax.rem(j, 2)
        x = mx + side * (3 - 2 * mx)
        to = lax.rem(mz + dz, 4) * 16 + lax.rem(my + dy, 4) * 4 + x
        return sp_copy(pk.at[to // 2], own.at[me], a_send.at[i], own_sem.at[me], to)

    def start_direct(i, _):
        direct_send(i).start()
        return 0

    lax.fori_loop(1, 32, start_direct, 0)
    stat_copy = tp_copy(stat_send, stat_recv, s_send, s_recv, peer)
    stat_copy.start()

    def gather(group, axis, part):
        def at(d):
            z, y, x = mz, my, mx
            if axis == 0:
                z = lax.rem(mz + d, 4)
            elif axis == 1:
                y = lax.rem(my + d, 4)
            else:
                x = lax.rem(mx + d, 4)
            return z, y, x

        def copy(d, send):
            z, y, x = at(0) if send else at(4 - d)
            to_z, to_y, to_x = at(d)
            block = proj.at[part(z, y, x)]
            return sp_copy(
                block, block, g_send.at[group, d - 1], g_recv.at[group, d - 1],
                to_z * 16 + to_y * 4 + to_x,
            )

        def start():
            for d in (1, 3, 2):
                copy(d, True).start()

        def take():
            for d in (1, 3, 2):
                copy(d, False).wait_recv()

        def sent():
            for d in (1, 3, 2):
                copy(d, True).wait_send()

        return start, take, sent

    every = slice(None)
    low, mid_cols, high = pl.ds(0, 256), pl.ds(256, 512), pl.ds(768, 256)
    first_hop = (
        gather(0, 2, lambda z, y, x: (z, y, x, every, pl.ds(0, 768))),
        gather(1, 1, lambda z, y, x: (z, y, x, every, high)),
    )
    second_hop = (
        gather(2, 1, lambda z, y, x: (z, y, every, every, low)),
        gather(3, 0, lambda z, y, x: (z, y, every, every, mid_cols)),
        gather(4, 0, lambda z, y, x: (z, every, x, every, high)),
    )
    third_hop = (
        gather(5, 0, lambda z, y, x: (z, every, every, every, low)),
        gather(6, 1, lambda z, y, x: (every, y, every, every, mid_cols)),
        gather(7, 2, lambda z, y, x: (every, every, x, every, high)),
    )
    for start, _, _ in first_hop:
        start()

    stat_copy.wait_recv()
    both = stat_send[...] + stat_recv[...]
    row_mean = both[:, 0:1] / D
    row_var = both[:, 1:2] / D - row_mean * row_mean
    inv_std = lax.rsqrt(row_var + 1e-06)
    stats[...] = jnp.where(lane == 0, row_mean, inv_std)
    scaled_z = (values - row_mean) * inv_std * gain[...]
    act[pl.ds(mz, 1)] = (scaled_z * jax.nn.sigmoid(scaled_z)).astype(BF16)[None]

    def act_copy(d, send):
        z = mz if send else lax.rem(mz + 4 - d, 4)
        return sp_copy(
            act.at[z], act.at[z], t_send.at[d - 1], t_recv.at[d - 1],
            lax.rem(mz + d, 4) * 16 + lax.rem(me, 16),
        )

    def source(k, j, near):
        dz, dy, side = gray(k), gray(j // 2), lax.rem(j, 2)
        x = mx + side * (3 - 2 * mx)
        twin_x = x + 1 - 2 * lax.rem(x, 2)
        x = x if near else twin_x
        return lax.rem(mz - dz + 4, 4) * 16 + lax.rem(my - dy + 4, 4) * 4 + x

    def twin_copy(i):
        s = source(i // 8, lax.rem(i, 8), True)
        return sp_copy(own.at[s], own.at[s], b_send.at[i], own_sem.at[s], twin)

    def core_copy(s):
        return tp_copy(own.at[s], oth.at[s], c_send.at[s], oth_sem.at[s], peer)

    def arrived(s):
        return sp_copy(own.at[s], own.at[s], c_send.at[s], own_sem.at[s], twin)

    def take_direct(k):
        def one(j, _):
            s = source(k, j, True)

            @pl.when(k * 8 + j != 0)
            def _():
                arrived(s).wait_recv()

            twin_copy(k * 8 + j).start()
            core_copy(s).start()
            return 0

        lax.fori_loop(0, 8, one, 0)

    def take_twin(k):
        def one(j, _):
            s = source(k, j, False)
            arrived(s).wait_recv()
            core_copy(s).start()
            return 0

        lax.fori_loop(0, 8, one, 0)

    def part_copy(z):
        return tp_copy(
            psend.at[pl.ds(z * 16, 16)], precv.at[pl.ds(z * 16, 16)],
            e_send.at[z], e_recv.at[z], peer,
        )

    def slot(s):
        return lax.rem(s, 2) * 32 + s // 2

    def ret_copy(s):
        return sp_copy(pown.at[s], ret.at[slot(me)], r_send.at[s], r_recv.at[me], s)

    def ret_arrived(s):
        return sp_copy(pown.at[s], ret.at[slot(s)], r_send.at[s], r_recv.at[s], s)

    def plane(k):
        return lax.rem(mz - gray(k) + 4, 4)

    def compute(k):
        z = plane(k)

        def wait_other(j, _):
            tp_copy(
                own.at[z * 16 + j], oth.at[z * 16 + j],
                c_send.at[z * 16 + j], oth_sem.at[z * 16 + j], peer,
            ).wait_recv()
            return 0

        lax.fori_loop(0, 16, wait_other, 0)
        base = pl.multiple_of(z * 192, 64)
        for buf, half in ((own, tp), (oth, peer)):
            block = buf[pl.ds(z * 16, 16)].reshape(128, 3072)
            left = pl.multiple_of(half * HALF, HALF)
            mid = pl.multiple_of(half * HALF + 512, 512)
            xs[pl.ds(base, 128), pl.ds(left, HALF)] = block[:, :HALF]
            ps[pl.ds(base, 128), pl.ds(left, HALF)] = block[:, HALF : 2 * HALF]
            rest = block[:, 2 * HALF :]
            first = nn(sel_a[...], rest).astype(BF16)
            second = nn(sel_b[...], rest).astype(BF16)
            low = pl.multiple_of(base + 128, 64)
            xs[pl.ds(low, 64), pl.ds(left, 512)] = first[:, :512]
            xs[pl.ds(low, 64), pl.ds(mid, 512)] = second[:, :512]
            ps[pl.ds(low, 64), pl.ds(left, 512)] = first[:, 512:]
            ps[pl.ds(low, 64), pl.ds(mid, 512)] = second[:, 512:]
        x = xs[pl.ds(base, 192), :]
        p = ps[pl.ds(base, 192), :]
        g = nn(x, wg[...])
        u = nn(x, wu[...])
        dh = nt(p, wd[...])
        sig = jax.nn.sigmoid(g)
        silu = g * sig
        acts[pl.ds(base, 192), :] = (silu * u).astype(BF16)
        dg = (dh * u * sig * (1.0 + g * (1.0 - sig))).astype(BF16)
        du = (dh * silu).astype(BF16)
        dgs[pl.ds(base, 192), :] = dg
        dus[pl.ds(base, 192), :] = du
        for out, half in ((psend, peer), (pown, tp)):
            rows = pl.ds(pl.multiple_of(half * HALF, HALF), HALF)
            back = nt(dg, wg[rows, :]) + nt(du, wu[rows, :])
            back = back.astype(BF16)
            out[pl.ds(z * 16, 16), :, :HALF] = back[:128].reshape(16, 8, HALF)
            rest = tn(sel_a[...], back[128:, :512]) + tn(sel_b[...], back[128:, 512:])
            out[pl.ds(z * 16, 16), :, HALF:] = rest.astype(BF16).reshape(16, 8, 512)
            if half is peer:
                part_copy(z).start()

    def give_back(k):
        z = plane(k)
        part_copy(z).wait_recv()
        block = pl.ds(z * 16, 16)
        pown[block] = (pown[block].astype(F32) + precv[block].astype(F32)).astype(BF16)

        def one(j, _):
            s = z * 16 + lax.rem(lax.rem(me, 16) + j, 16)

            @pl.when(s != me)
            def _():
                ret_copy(s).start()

            return 0

        lax.fori_loop(0, 16, one, 0)

    take_direct(0)
    take_direct(1)
    for d in (1, 3, 2):
        act_copy(d, True).start()
    for _, take, _ in first_hop:
        take()
    for start, _, _ in second_hop:
        start()
    take_twin(0)
    for copy in loads:
        copy.wait()

    def step(k, _):
        @pl.when(k < 2)
        def _():
            take_direct(k + 2)

        compute(k)

        @pl.when(k < 3)
        def _():
            take_twin(k + 1)

        @pl.when(k > 0)
        def _():
            give_back(k - 1)

        @pl.when(k == 0)
        def _():
            for _, take, _ in second_hop:
                take()
            for start, _, _ in third_hop[:2]:
                start()

        return 0

    lax.fori_loop(0, 4, step, 0)
    give_back(3)
    ret[pl.ds(slot(me), 1)] = pown[pl.ds(me, 1)]
    third_hop[2][0]()

    def weight_grads(i, _):
        cols = pl.ds(pl.multiple_of(i * 256, 256), 256)
        rows = xs[:, cols].T
        wg[cols, :] = nn(rows, dgs[...]).astype(BF16)
        wu[cols, :] = nn(rows, dus[...]).astype(BF16)
        return 0

    lax.fori_loop(0, 8, weight_grads, 0)

    def down_grads(i, _):
        cols = pl.ds(pl.multiple_of(i * 128, 128), 128)
        wd[cols, :] = nn(acts[:, cols].T, ps[...]).astype(BF16)
        return 0

    lax.fori_loop(0, 7, down_grads, 0)
    taps_f[pl.ds(0, 31), :] = taps[...].astype(F32)

    def await_return(s, _):
        @pl.when(s != me)
        def _():
            ret_arrived(s).wait_recv()

        return 0

    lax.fori_loop(0, 64, await_return, 0)
    contrib = jnp.zeros((128, HALF), F32)
    halves = []
    for h in range(2):
        block = ret[pl.ds(h * 32, 32)].reshape(256, 1536)
        contrib = contrib + tn(table[6], block[:, :HALF])
        halves.append(block[:, HALF:])
    left = tn(table[7], halves[0]) + tn(table[7], halves[1])
    right = tn(table[8], halves[0]) + tn(table[8], halves[1])
    left = (out_grad[:, :512].astype(F32) + (contrib[:, :512] + left)).astype(BF16)
    right = (out_grad[:, 512:].astype(F32) + (contrib[:, 512:] + right)).astype(BF16)
    gs[pl.ds(2 * tp, 1)] = left[None]
    gs[pl.ds(2 * tp + 1, 1)] = right[None]

    def stream_copy(tp_of):
        rows = pl.ds(2 * tp_of, 2)
        return tp_copy(gs.at[rows], gs.at[rows], q_send, q_recv, peer)

    def plane_copy(z, core, i):
        return pltpu.make_async_remote_copy(
            src_ref=gs.at[z], dst_ref=gz.at[mz],
            send_sem=z_send.at[i, core], recv_sem=z_recv.at[mz],
            device_id={"sp": z * 16 + here, "tp": core}, device_id_type=MESH,
        )

    def plane_arrived(z):
        return sp_copy(gz.at[z], gz.at[z], z_send.at[0, 0], z_recv.at[z], z * 16 + here)

    stream_copy(tp).start()
    for i in range(2):
        z = 2 * tp + i

        @pl.when(z != mz)
        def _():
            plane_copy(z, 0, i).start()
            plane_copy(z, 1, i).start()

    for d in (1, 2, 3):
        act_copy(d, False).wait_recv()

    def weights(z):
        return proj[pl.ds(z, 1)].reshape(512, HALF)

    for _, take, _ in third_hop:
        take()
    grad_act = nn(left, weights(2 * tp)) + nn(right, weights(2 * tp + 1))
    stream_copy(peer).wait_recv()
    mine = gs[pl.ds(mz, 1)].reshape(128, 512)
    total = tn(mine, act[pl.ds(mz, 1)].reshape(128, HALF))
    for d in (1, 3, 2):
        z = lax.rem(mz + d, 4)
        plane_arrived(z).wait_recv()
        total = total + tn(gz[pl.ds(z, 1)].reshape(128, 512), act[pl.ds(z, 1)].reshape(128, HALF))
    part[...] = total.astype(BF16).reshape(16, 32, HALF)

    def proj_copy(d):
        q = lax.rem(here + d, 16)
        return sp_copy(part.at[q], parts.at[here], p_send.at[d], p_recv.at[here], mz * 16 + q)

    def part_arrived(q):
        return sp_copy(parts.at[q], parts.at[q], p_send.at[0], p_recv.at[q], mz * 16 + q)

    def start_part(d, _):
        proj_copy(d).start()
        return 0

    other = gs[pl.ds(2 * peer, 2)]
    grad_act = grad_act + nn(other[0], weights(2 * peer)) + nn(other[1], weights(2 * peer + 1))
    lax.fori_loop(1, 16, start_part, 0)

    row_mean, inv_std = stats[:, 0:1], stats[:, 1:2]
    normed = (conv[...].astype(F32) - row_mean) * inv_std
    scaled_z = normed * gain[...]
    z_sig = jax.nn.sigmoid(scaled_z)
    grad_normed = grad_act * z_sig * (1.0 + scaled_z * (1.0 - z_sig)) * gain[...]
    sum_send[...] = jnp.where(
        lane == 0,
        jnp.sum(grad_normed, axis=1, keepdims=True),
        jnp.sum(grad_normed * normed, axis=1, keepdims=True),
    )
    sum_copy = tp_copy(sum_send, sum_recv, u_send, u_recv, peer)
    sum_copy.start()
    sum_copy.wait_recv()
    both = sum_send[...] + sum_recv[...]
    grad_conv = inv_std * (grad_normed - both[:, 0:1] / D - normed * (both[:, 1:2] / D))
    ext[pl.ds(0, 128), :] = grad_conv.astype(BF16).astype(F32)

    def reach_copy(to):
        return sp_copy(ext.at[pl.ds(0, 32)], ext.at[pl.ds(128, 32)], h_send, h_recv, to)

    @pl.when(me == 63)
    def _():
        ext[pl.ds(128, 32), :] = jnp.zeros((32, HALF), F32)

    @pl.when(me > 0)
    def _():
        reach_copy(me - 1).start()

    parts[pl.ds(here, 1)] = part[pl.ds(here, 1)]

    @pl.when(me < 63)
    def _():
        reach_copy(me + 1).wait_recv()

    def columns(c, _):
        cols = pl.ds(pl.multiple_of(c * 128, 128), 128)
        acc = jnp.zeros((128, 128), F32)
        for k in range(31):
            acc = acc + taps_f[pl.ds(k, 1), cols] * ext[pl.ds(k, 128), cols]
        gin_out[:, cols] = acc.astype(BF16)
        return 0

    lax.fori_loop(0, 8, columns, 0)

    def wait_part(d, _):
        part_arrived(lax.rem(here + d, 16)).wait_recv()
        return 0

    lax.fori_loop(1, 16, wait_part, 0)
    result = parts[0].astype(F32)
    for q in range(1, 16):
        result = result + parts[q].astype(F32)
    gproj_out[...] = result

    def sent_part(d, _):
        proj_copy(d).wait_send()
        return 0

    lax.fori_loop(1, 16, sent_part, 0)
    stream_copy(tp).wait_send()
    sum_copy.wait_send()
    for i in range(2):
        z = 2 * tp + i

        @pl.when(z != mz)
        def _():
            plane_copy(z, 0, i).wait_send()
            plane_copy(z, 1, i).wait_send()

    @pl.when(me > 0)
    def _():
        reach_copy(me - 1).wait_send()

    def finish_sends(i, _):
        @pl.when(i > 0)
        def _():
            direct_send(i).wait_send()

        twin_copy(i).wait_send()
        return 0

    lax.fori_loop(0, 32, finish_sends, 0)

    def finish(s, _):
        core_copy(s).wait_send()

        @pl.when(s != me)
        def _():
            ret_copy(s).wait_send()

        return 0

    lax.fori_loop(0, 64, finish, 0)
    for z in range(4):
        part_copy(z).wait_send()
    for _, _, sent in first_hop + second_hop + third_hop:
        sent()
    for d in (1, 2, 3):
        act_copy(d, True).wait_send()
    stat_copy.wait_send()
def on_device(
    conv_out, ln_gain, taps, proj_weight, stream_mid, out_grad,
    routes, route_probs, gate_slabs, up_slabs, down_slabs,
):
    hidden = gate_slabs.shape[2]
    rows = 768
    dma = pltpu.SemaphoreType.DMA
    vmem = pltpu.VMEM
    slots = vmem((64, 8, 1536), BF16)
    grad_input, grad_proj, grad_gate, grad_up, grad_down = pl.pallas_call(
        layer_kernel,
        out_shape=[
            jax.ShapeDtypeStruct((128, HALF), BF16),
            jax.ShapeDtypeStruct((32, HALF), F32),
            jax.ShapeDtypeStruct((D, hidden), BF16),
            jax.ShapeDtypeStruct((D, hidden), BF16),
            jax.ShapeDtypeStruct((hidden, D), BF16),
        ],
        in_specs=[pl.BlockSpec(memory_space=pltpu.VMEM)] * 7 + [pl.BlockSpec(memory_space=pl.ANY)] * 4,
        out_specs=[pl.BlockSpec(memory_space=pltpu.VMEM)] * 5,
        scratch_shapes=[
            vmem((32, 8, 3072), BF16),
            vmem((64, 8, 3072), BF16), vmem((64, 8, 3072), BF16),
            vmem((rows, D), BF16), vmem((rows, D), BF16),
            vmem((rows, hidden), BF16), vmem((rows, hidden), BF16), vmem((rows, hidden), BF16),
            slots, slots, slots, slots,
            vmem((9, 256, 128), BF16), vmem((64, 128), BF16), vmem((64, 128), BF16),
            vmem((4, 4, 4, 32, HALF), BF16), vmem((4, 128, HALF), BF16),
            vmem((128, 128), F32), vmem((128, 128), F32), vmem((128, 128), F32),
            vmem((4, 128, 512), BF16), vmem((4, 128, 512), BF16),
            vmem((16, 32, HALF), BF16), vmem((16, 32, HALF), BF16),
            vmem((160, HALF), F32),
            vmem((128, 128), F32), vmem((128, 128), F32), vmem((32, HALF), F32),
            dma((4,)), dma((32,)), dma((32,)), dma((64,)), dma((64,)), dma((64,)),
            dma((4,)), dma((4,)), dma((64,)), dma((64,)),
            dma((8, 3)), dma((8, 3)), dma, dma, dma((3,)), dma((3,)),
            dma, dma, dma((2, 2)), dma((4,)), dma((16,)), dma((16,)), dma, dma, dma, dma,
        ],
        compiler_params=pltpu.CompilerParams(
            collective_id=0, has_side_effects=True, vmem_limit_bytes=VMEM_BYTES
        ),
        name="layer",
    )(
        routes.T, route_probs.T, stream_mid, out_grad, conv_out, ln_gain[None, :], taps,
        gate_slabs[0], up_slabs[0], down_slabs[0], proj_weight,
    )
    return grad_input, grad_proj, grad_gate[None], grad_up[None], grad_down[None]


def solution(mesh):
    return jax.shard_map(
        on_device,
        mesh=mesh,
        in_specs=(
            P("sp", "tp"), P("tp"), P(None, "tp"), P("sp", "tp"), P("sp", "tp"), P("sp", "tp"),
            P("sp", None), P("sp", None), P("sp", None, "tp"), P("sp", None, "tp"), P("sp", "tp", None),
        ),
        out_specs=(
            P("sp", "tp"), P("sp", "tp"), P("sp", None, "tp"), P("sp", None, "tp"), P("sp", "tp", None),
        ),
        check_vma=False,
    )
```

time: 166 us -> 146 us (0.88)
  matrix products: 20.1 us -> 0 us
  local copies, waits for them, and re-layouts: 7.04 us -> 13.4 us
  other arithmetic: 4.77 us -> 0 us
    dot_general x10 -> x0, matrix products: 20.1 us -> none  [the longest x9 20 us: tn(): lax.dot_general(a, b, (((0,), (0,)), ((), ())), preferred_element_type=F32)]
    unnamed x28 -> x21, local copies, waits for them, and re-layouts: 7.04 us -> 13.4 us
    reduce_sum x3 -> x0, other arithmetic: 2.41 us -> none  [the longest x1 0.96 us: weights(): jnp.sum(t.astype(F32) * route_probs[:, :, None], axis=(0, 1))[:, None]]
    pallas_call x2 -> x1, Pallas kernels: 132 us -> 131 us  [on_device(): pl.pallas_call(layer_kernel, out_shape=[jax.ShapeDtypeStruct((128, HALF),...]
where the time goes in v3:
time: 146 us; the launch traced here: 145 us
  Pallas kernels  131 us (90%)
  local copies, waits for them, and re-layouts  13.4 us (9%)
    pallas_call x1, Pallas kernels, on_device(): pl.pallas_call(layer_kernel, out_shape=[jax.ShapeDtypeStruct((128, HALF),...  131 us
    unnamed x21, local copies, waits for them, and re-layouts  13.4 us

profile of v3, /device:TPU:1, one launch (start us, length us, event | category | flops | bytes accessed | tf_op | source)
XLA Modules:
  0.0 145.1 jit_solution(17338166792128582457)
XLA Ops:
  0.6 0.0 copy-start
  0.6 0.9 copy-done
  1.6 0.0 copy-start.1
  1.6 0.9 copy-done.1
  2.5 0.0 copy-start.2
  2.5 0.9 copy-done.2
  3.5 0.0 copy-start.3
  3.5 0.8 copy-done.3
  4.3 0.0 copy-start.4
  4.3 0.8 copy-done.4
  5.2 0.0 copy-start.5
  5.2 0.7 copy-done.5
  5.9 0.0 copy-start.6
  5.9 0.7 copy-done.6
  6.5 0.0 copy-start.7
  6.5 0.7 copy-done.7
  7.2 131.0 %layer.1 = (bf16[128,1024]{1,0:T(8,128)(2,1)S(1)}, f32[32,1024]{1,0:T(8,128)S(1)}, bf16[2048,896]{1,0:T(8,128)(2,1)S(1)}, bf16[2048,896]{1,0:T(8,128)(2,1)S(1)}, bf16[896,2048]{1,0:T(8,128)(2,1)S(1)}) custom-call(s32[2,128]{1,0:T(2,128)S(1)} %bitcast.13, f32[2,128]{1,0:T(2,128)S(1)} %bitcast.14, bf16[128,1024]{1,0:T(8,128)(2,1)S(1)} %copy-done, ...), custom_call_target="tpu_custom_call" | custom-call | tf_op jit(solution)/shard_map/layer/pallas_call | solution.py:589
  138.2 0.7 copy.21
  138.9 0.7 copy.22
  139.6 1.8 %copy.23 = bf16[1,2048,896]{2,1,0:T(8,128)(2,1)} copy(bf16[1,2048,896]{2,1,0:T(8,128)(2,1)S(1)} %bitcast.11) | data formatting | bytes 7340032
  141.4 1.8 %copy.24 = bf16[1,2048,896]{2,1,0:T(8,128)(2,1)} copy(bf16[1,2048,896]{2,1,0:T(8,128)(2,1)S(1)} %bitcast.10) | data formatting | bytes 7340032
  143.2 1.8 %copy.25 = bf16[1,896,2048]{2,1,0:T(8,128)(2,1)} copy(bf16[1,896,2048]{2,1,0:T(8,128)(2,1)S(1)} %bitcast.9) | data formatting | bytes 7340032
Async XLA Ops:
  0.6 1.0 copy-start
  1.6 0.9 copy-start.1
  2.5 0.9 copy-start.2
  3.5 0.8 copy-start.3
  4.3 0.8 copy-start.4
  5.2 0.7 copy-start.5
  5.9 0.7 copy-start.6
  6.5 0.7 copy-start.7

commit v4 on v3

--- a/solution.py
+++ b/solution.py
@@ -48,15 +48,17 @@
 
 
 def layer_kernel(
-    routes, probs, stream, out_grad, conv, gain, taps, wg_hbm, wu_hbm, wd_hbm, proj_hbm,
+    routes_hbm, probs_hbm, stream_hbm, out_grad_hbm, conv_hbm, gain_hbm, taps_hbm,
+    wg_hbm, wu_hbm, wd_hbm, proj_hbm,
     gin_out, gproj_out, wg, wu, wd,
+    routes, probs, stream, out_grad, conv, gain, taps,
     pk, own, oth, xs, ps, acts, dgs, dus, psend, precv, pown, ret,
     table, sel_a, sel_b, proj, act, stat_send, stat_recv, stats,
     gs, gz, part, parts, ext, sum_send, sum_recv, taps_f,
     w_sem, a_send, b_send, c_send, own_sem, oth_sem,
     e_send, e_recv, r_send, r_recv,
     g_send, g_recv, s_send, s_recv, t_send, t_recv,
-    q_send, q_recv, z_send, z_recv, p_send, p_recv, u_send, u_recv, h_send, h_recv,
+    i_sem, q_send, q_recv, z_send, z_recv, p_send, p_recv, u_send, u_recv, h_send, h_recv,
 ):
     me = lax.axis_index("sp")
     tp = lax.axis_index("tp")
@@ -68,6 +70,17 @@
         pltpu.make_async_copy(src, dst, w_sem.at[i])
         for i, (src, dst) in enumerate(((wg_hbm, wg), (wu_hbm, wu), (wd_hbm, wd)))
     ]
+    small = [
+        pltpu.make_async_copy(src, dst, i_sem.at[i])
+        for i, (src, dst) in enumerate(
+            (
+                (routes_hbm, routes), (probs_hbm, probs), (stream_hbm, stream),
+                (out_grad_hbm, out_grad), (conv_hbm, conv), (gain_hbm, gain), (taps_hbm, taps),
+            )
+        )
+    ]
+    for copy in small:
+        copy.start()
     proj_load = pltpu.make_async_copy(proj_hbm, proj.at[mz, my, mx], w_sem.at[3])
     proj_load.start()
     for copy in loads:
@@ -88,6 +101,9 @@
             barrier, inc=1, device_id={"sp": lax.rem(mz + d, 4) * 16 + here, "tp": peer},
             device_id_type=MESH,
         )
+
+    for copy in small:
+        copy.wait()
 
     expert = lax.broadcasted_iota(jnp.int32, (128, 128), 0)
     other = lax.broadcasted_iota(jnp.int32, (128, 128), 1)
@@ -146,7 +162,6 @@
         direct_send(i).start()
         return 0
 
-    lax.fori_loop(1, 32, start_direct, 0)
     stat_copy = tp_copy(stat_send, stat_recv, s_send, s_recv, peer)
     stat_copy.start()
 
@@ -202,6 +217,7 @@
     )
     for start, _, _ in first_hop:
         start()
+    lax.fori_loop(1, 32, start_direct, 0)
 
     stat_copy.wait_recv()
     both = stat_send[...] + stat_recv[...]
@@ -342,14 +358,18 @@
 
         lax.fori_loop(0, 16, one, 0)
 
-    take_direct(0)
-    take_direct(1)
-    for d in (1, 3, 2):
-        act_copy(d, True).start()
     for _, take, _ in first_hop:
         take()
     for start, _, _ in second_hop:
         start()
+    take_direct(0)
+    for d in (1, 3, 2):
+        act_copy(d, True).start()
+    take_direct(1)
+    for _, take, _ in second_hop:
+        take()
+    for start, _, _ in third_hop[:2]:
+        start()
     take_twin(0)
     for copy in loads:
         copy.wait()
@@ -359,22 +379,16 @@
         def _():
             take_direct(k + 2)
 
+        @pl.when(k > 0)
+        def _():
+            give_back(k - 1)
+
         compute(k)
 
         @pl.when(k < 3)
         def _():
             take_twin(k + 1)
 
-        @pl.when(k > 0)
-        def _():
-            give_back(k - 1)
-
-        @pl.when(k == 0)
-        def _():
-            for _, take, _ in second_hop:
-                take()
-            for start, _, _ in third_hop[:2]:
-                start()
 
         return 0
 
@@ -595,9 +609,12 @@
             jax.ShapeDtypeStruct((D, hidden), BF16),
             jax.ShapeDtypeStruct((hidden, D), BF16),
         ],
-        in_specs=[pl.BlockSpec(memory_space=pltpu.VMEM)] * 7 + [pl.BlockSpec(memory_space=pl.ANY)] * 4,
+        in_specs=[pl.BlockSpec(memory_space=pl.ANY)] * 11,
         out_specs=[pl.BlockSpec(memory_space=pltpu.VMEM)] * 5,
         scratch_shapes=[
+            vmem((2, 128), jnp.int32), vmem((2, 128), F32),
+            vmem((128, HALF), BF16), vmem((128, HALF), BF16), vmem((128, HALF), BF16),
+            vmem((1, HALF), F32), vmem((31, HALF), BF16),
             vmem((32, 8, 3072), BF16),
             vmem((64, 8, 3072), BF16), vmem((64, 8, 3072), BF16),
             vmem((rows, D), BF16), vmem((rows, D), BF16),
@@ -613,15 +630,20 @@
             dma((4,)), dma((32,)), dma((32,)), dma((64,)), dma((64,)), dma((64,)),
             dma((4,)), dma((4,)), dma((64,)), dma((64,)),
             dma((8, 3)), dma((8, 3)), dma, dma, dma((3,)), dma((3,)),
-            dma, dma, dma((2, 2)), dma((4,)), dma((16,)), dma((16,)), dma, dma, dma, dma,
+            dma((7,)), dma, dma, dma((2, 2)), dma((4,)), dma((16,)), dma((16,)), dma, dma, dma, dma,
         ],
         compiler_params=pltpu.CompilerParams(
             collective_id=0, has_side_effects=True, vmem_limit_bytes=VMEM_BYTES
         ),
         name="layer",
     )(
-        routes.T, route_probs.T, stream_mid, out_grad, conv_out, ln_gain[None, :], taps,
-        gate_slabs[0], up_slabs[0], down_slabs[0], proj_weight,
+        *(
+            pltpu.with_memory_space_constraint(a, pltpu.HBM)
+            for a in (
+                routes.T, route_probs.T, stream_mid, out_grad, conv_out, ln_gain[None, :], taps,
+                gate_slabs[0], up_slabs[0], down_slabs[0], proj_weight,
+            )
+        )
     )
     return grad_input, grad_proj, grad_gate[None], grad_up[None], grad_down[None]
 

time: 146 us -> 126 us (0.86)
  Pallas kernels: 131 us -> 119 us
  local copies, waits for them, and re-layouts: 13.4 us -> 6.87 us
    pallas_call x1, Pallas kernels: 131 us -> 119 us  [on_device(): pl.pallas_call(layer_kernel, out_shape=[jax.ShapeDtypeStruct((128, HALF),...]
    unnamed x21 -> x5, local copies, waits for them, and re-layouts: 13.4 us -> 6.87 us
where the time goes in v4:
time: 126 us
  Pallas kernels  119 us (94%)
  local copies, waits for them, and re-layouts  6.87 us (5%)
    pallas_call x1, Pallas kernels, on_device(): pl.pallas_call(layer_kernel, out_shape=[jax.ShapeDtypeStruct((128, HALF),...  119 us
    unnamed x5, local copies, waits for them, and re-layouts  6.87 us

profile of v4, /device:TPU:1, one launch (start us, length us, event | category | flops | bytes accessed | tf_op | source)
XLA Modules:
  0.0 126.1 jit_solution(13242596265406450427)
XLA Ops:
  0.6 118.6 %layer.1 = (bf16[128,1024]{1,0:T(8,128)(2,1)S(1)}, f32[32,1024]{1,0:T(8,128)S(1)}, bf16[2048,896]{1,0:T(8,128)(2,1)S(1)}, bf16[2048,896]{1,0:T(8,128)(2,1)S(1)}, bf16[896,2048]{1,0:T(8,128)(2,1)S(1)}) custom-call(s32[2,128]{1,0:T(2,128)} %bitcast.16, f32[2,128]{1,0:T(2,128)} %bitcast.17, bf16[128,1024]{1,0:T(8,128)(2,1)} %stream_hbm.1, ...), custom_call_target="tpu_custom_call" | custom-call | tf_op jit(solution)/shard_map/layer/pallas_call | solution.py:603
  119.2 0.7 copy.21
  119.9 0.7 copy.22
  120.6 1.8 %copy.23 = bf16[1,2048,896]{2,1,0:T(8,128)(2,1)} copy(bf16[1,2048,896]{2,1,0:T(8,128)(2,1)S(1)} %bitcast.11) | data formatting | bytes 7340032
  122.4 1.8 %copy.24 = bf16[1,2048,896]{2,1,0:T(8,128)(2,1)} copy(bf16[1,2048,896]{2,1,0:T(8,128)(2,1)S(1)} %bitcast.10) | data formatting | bytes 7340032
  124.3 1.8 %copy.25 = bf16[1,896,2048]{2,1,0:T(8,128)(2,1)} copy(bf16[1,896,2048]{2,1,0:T(8,128)(2,1)S(1)} %bitcast.9) | data formatting | bytes 7340032

commit v5 on v4

--- a/solution.py
+++ b/solution.py
@@ -126,15 +126,85 @@
     pk[:, :, :HALF] = nn(table[6], stream[...]).astype(BF16).reshape(shape)
     rest = nn(table[7], stream[:, :512]) + nn(table[8], stream[:, 512:])
     pk[:, :, 2 * HALF : 2 * HALF + 512] = rest.astype(BF16).reshape(32, 8, 512)
-    grads = []
-    for j in range(2):
-        prob = jnp.broadcast_to(probs[j : j + 1, :], (128, 128)).T[:, 0:1]
-        grads.append((out_grad[...].astype(F32) * prob).astype(BF16))
-    near = nn(table[0], grads[0]) + nn(table[3], grads[1])
+    p_main = table[0].astype(F32) * probs[0:1, :] + table[3].astype(F32) * probs[1:2, :]
+    p_main = jnp.sum(p_main, axis=1, keepdims=True)
+    near = nn(table[6], out_grad[...]) * p_main
     pk[:, :, HALF : 2 * HALF] = near.astype(BF16).reshape(shape)
-    rest = nn(table[1], grads[0][:, :512]) + nn(table[4], grads[1][:, :512])
-    rest = rest + nn(table[2], grads[0][:, 512:]) + nn(table[5], grads[1][:, 512:])
-    pk[:, :, 2 * HALF + 512 :] = rest.astype(BF16).reshape(32, 8, 512)
+    p_rest = (table[1] + table[2]).astype(F32) * probs[0:1, :]
+    p_rest = p_rest + (table[4] + table[5]).astype(F32) * probs[1:2, :]
+    p_rest = jnp.sum(p_rest, axis=1, keepdims=True)
+    rest = nn(table[7], out_grad[:, :512]) + nn(table[8], out_grad[:, 512:])
+    pk[:, :, 2 * HALF + 512 :] = (rest * p_rest).astype(BF16).reshape(32, 8, 512)
+
+    proj_load.wait()
+
+    pl.semaphore_wait(barrier, 67)
+
+    def direct_send(i):
+        k, j = i // 8, lax.rem(i, 8)
+        dz, dy, side = gray(k), gray(j // 2), lax.rem(j, 2)
+        x = mx + side * (3 - 2 * mx)
+        to = lax.rem(mz + dz, 4) * 16 + lax.rem(my + dy, 4) * 4 + x
+        return sp_copy(pk.at[to // 2], own.at[me], a_send.at[i], own_sem.at[me], to)
+
+    def start_direct(i, _):
+        direct_send(i).start()
+        return 0
+
+
+    def gather(group, axis, part):
+        def at(d):
+            z, y, x = mz, my, mx
+            if axis == 0:
+                z = lax.rem(mz + d, 4)
+            elif axis == 1:
+                y = lax.rem(my + d, 4)
+            else:
+                x = lax.rem(mx + d, 4)
+            return z, y, x
+
+        def copy(d, send):
+            z, y, x = at(0) if send else at(4 - d)
+            to_z, to_y, to_x = at(d)
+            block = proj.at[part(z, y, x)]
+            return sp_copy(
+                block, block, g_send.at[group, d - 1], g_recv.at[group, d - 1],
+                to_z * 16 + to_y * 4 + to_x,
+            )
+
+        def start():
+            for d in (1, 3, 2):
+                copy(d, True).start()
+
+        def take():
+            for d in (1, 3, 2):
+                copy(d, False).wait_recv()
+
+        def sent():
+            for d in (1, 3, 2):
+                copy(d, True).wait_send()
+
+        return start, take, sent
+
+    every = slice(None)
+    low, mid_cols, high = pl.ds(0, 384), pl.ds(384, 512), pl.ds(896, 128)
+    first_hop = (
+        gather(0, 2, lambda z, y, x: (z, y, x, every, pl.ds(0, 896))),
+        gather(1, 1, lambda z, y, x: (z, y, x, every, high)),
+    )
+    second_hop = (
+        gather(2, 1, lambda z, y, x: (z, y, every, every, low)),
+        gather(3, 0, lambda z, y, x: (z, y, every, every, mid_cols)),
+        gather(4, 0, lambda z, y, x: (z, every, x, every, high)),
+    )
+    third_hop = (
+        gather(5, 0, lambda z, y, x: (z, every, every, every, low)),
+        gather(6, 1, lambda z, y, x: (every, y, every, every, mid_cols)),
+        gather(7, 2, lambda z, y, x: (every, every, x, every, high)),
+    )
+    for start, _, _ in first_hop:
+        start()
+    lax.fori_loop(1, 32, start_direct, 0)
 
     row = lax.broadcasted_iota(jnp.int32, (64, 128), 0)
     col = lax.broadcasted_iota(jnp.int32, (64, 128), 1)
@@ -147,77 +217,8 @@
     total = jnp.sum(values, axis=1, keepdims=True)
     squares = jnp.sum(values * values, axis=1, keepdims=True)
     stat_send[...] = jnp.where(lane == 0, total, squares)
-    proj_load.wait()
-
-    pl.semaphore_wait(barrier, 67)
-
-    def direct_send(i):
-        k, j = i // 8, lax.rem(i, 8)
-        dz, dy, side = gray(k), gray(j // 2), lax.rem(j, 2)
-        x = mx + side * (3 - 2 * mx)
-        to = lax.rem(mz + dz, 4) * 16 + lax.rem(my + dy, 4) * 4 + x
-        return sp_copy(pk.at[to // 2], own.at[me], a_send.at[i], own_sem.at[me], to)
-
-    def start_direct(i, _):
-        direct_send(i).start()
-        return 0
-
     stat_copy = tp_copy(stat_send, stat_recv, s_send, s_recv, peer)
     stat_copy.start()
-
-    def gather(group, axis, part):
-        def at(d):
-            z, y, x = mz, my, mx
-            if axis == 0:
-                z = lax.rem(mz + d, 4)
-            elif axis == 1:
-                y = lax.rem(my + d, 4)
-            else:
-                x = lax.rem(mx + d, 4)
-            return z, y, x
-
-        def copy(d, send):
-            z, y, x = at(0) if send else at(4 - d)
-            to_z, to_y, to_x = at(d)
-            block = proj.at[part(z, y, x)]
-            return sp_copy(
-                block, block, g_send.at[group, d - 1], g_recv.at[group, d - 1],
-                to_z * 16 + to_y * 4 + to_x,
-            )
-
-        def start():
-            for d in (1, 3, 2):
-                copy(d, True).start()
-
-        def take():
-            for d in (1, 3, 2):
-                copy(d, False).wait_recv()
-
-        def sent():
-            for d in (1, 3, 2):
-                copy(d, True).wait_send()
-
-        return start, take, sent
-
-    every = slice(None)
-    low, mid_cols, high = pl.ds(0, 256), pl.ds(256, 512), pl.ds(768, 256)
-    first_hop = (
-        gather(0, 2, lambda z, y, x: (z, y, x, every, pl.ds(0, 768))),
-        gather(1, 1, lambda z, y, x: (z, y, x, every, high)),
-    )
-    second_hop = (
-        gather(2, 1, lambda z, y, x: (z, y, every, every, low)),
-        gather(3, 0, lambda z, y, x: (z, y, every, every, mid_cols)),
-        gather(4, 0, lambda z, y, x: (z, every, x, every, high)),
-    )
-    third_hop = (
-        gather(5, 0, lambda z, y, x: (z, every, every, every, low)),
-        gather(6, 1, lambda z, y, x: (every, y, every, every, mid_cols)),
-        gather(7, 2, lambda z, y, x: (every, every, x, every, high)),
-    )
-    for start, _, _ in first_hop:
-        start()
-    lax.fori_loop(1, 32, start_direct, 0)
 
     stat_copy.wait_recv()
     both = stat_send[...] + stat_recv[...]
@@ -591,6 +592,15 @@
     for d in (1, 2, 3):
         act_copy(d, True).wait_send()
     stat_copy.wait_send()
+def store_kernel(*refs):
+    sems = refs[10]
+    copies = [pltpu.make_async_copy(refs[i], refs[5 + i], sems.at[i]) for i in range(5)]
+    for copy in copies:
+        copy.start()
+    for copy in copies:
+        copy.wait()
+
+
 def on_device(
     conv_out, ln_gain, taps, proj_weight, stream_mid, out_grad,
     routes, route_probs, gate_slabs, up_slabs, down_slabs,
@@ -645,6 +655,16 @@
             )
         )
     )
+    done = (grad_input, grad_proj, grad_gate, grad_up, grad_down)
+    grad_input, grad_proj, grad_gate, grad_up, grad_down = pl.pallas_call(
+        store_kernel,
+        out_shape=[jax.ShapeDtypeStruct(a.shape, a.dtype) for a in done],
+        in_specs=[pl.BlockSpec(memory_space=pltpu.VMEM)] * 5,
+        out_specs=[pl.BlockSpec(memory_space=pl.ANY)] * 5,
+        scratch_shapes=[dma((5,))],
+        compiler_params=pltpu.CompilerParams(vmem_limit_bytes=1024 * 1024),
+        name="store",
+    )(*done)
     return grad_input, grad_proj, grad_gate[None], grad_up[None], grad_down[None]
 
 

time: 126 us -> 122 us (0.968)
  local copies, waits for them, and re-layouts: 6.87 us -> 0 us
  Pallas kernels: 119 us -> 121 us
    unnamed x5 -> x0, local copies, waits for them, and re-layouts: 6.87 us -> none
    pallas_call x0 -> x1, Pallas kernels: none -> 4.43 us  [on_device(): pl.pallas_call(store_kernel, out_shape=[jax.ShapeDtypeStruct(a.shape, a.d...]
    pallas_call x1, Pallas kernels: 119 us -> 117 us  [on_device(): pl.pallas_call(layer_kernel, out_shape=[jax.ShapeDtypeStruct((128, HALF),...]
where the time goes in v5:
time: 122 us
  Pallas kernels  121 us (99%)
    pallas_call x1, Pallas kernels, on_device(): pl.pallas_call(layer_kernel, out_shape=[jax.ShapeDtypeStruct((128, HALF),...  117 us
    pallas_call x1, Pallas kernels, on_device(): pl.pallas_call(store_kernel, out_shape=[jax.ShapeDtypeStruct(a.shape, a.d...  4.43 us

profile of v5, /device:TPU:1, one launch (start us, length us, event | category | flops | bytes accessed | tf_op | source)
XLA Modules:
  0.0 122.1 jit_solution(13011873801746902417)
XLA Ops:
  0.6 117.1 %layer.1 = (bf16[128,1024]{1,0:T(8,128)(2,1)S(1)}, f32[32,1024]{1,0:T(8,128)S(1)}, bf16[2048,896]{1,0:T(8,128)(2,1)S(1)}, bf16[2048,896]{1,0:T(8,128)(2,1)S(1)}, bf16[896,2048]{1,0:T(8,128)(2,1)S(1)}) custom-call(s32[2,128]{1,0:T(2,128)} %bitcast.13, f32[2,128]{1,0:T(2,128)} %bitcast.14, bf16[128,1024]{1,0:T(8,128)(2,1)} %stream_hbm.1, ...), custom_call_target="tpu_custom_call" | custom-call | tf_op jit(solution)/shard_map/layer/pallas_call | solution.py:613
  117.7 4.4 %store.1 = (bf16[128,1024]{1,0:T(8,128)(2,1)}, f32[32,1024]{1,0:T(8,128)}, bf16[2048,896]{1,0:T(8,128)(2,1)}, bf16[2048,896]{1,0:T(8,128)(2,1)}, bf16[896,2048]{1,0:T(8,128)(2,1)}) custom-call(bf16[128,1024]{1,0:T(8,128)(2,1)S(1)} %get-tuple-element.15.refs_0_, f32[32,1024]{1,0:T(8,128)S(1)} %get-tuple-element.16.refs_1_, ...), custom_call_target="tpu_custom_call" | custom-call | tf_op jit(solution)/shard_map/store/pallas_call | solution.py:659

commit v6 on v5

--- a/solution.py
+++ b/solution.py
@@ -43,8 +43,8 @@
     )
 
 
-def gray(k):
-    return lax.rem(k + k // 2 - 2 * (k // 3), 4)
+def order(k):
+    return lax.rem(k * 2, 4) + k // 2
 
 
 def layer_kernel(
@@ -142,7 +142,7 @@
 
     def direct_send(i):
         k, j = i // 8, lax.rem(i, 8)
-        dz, dy, side = gray(k), gray(j // 2), lax.rem(j, 2)
+        dz, dy, side = order(k), order(j // 2), lax.rem(j, 2)
         x = mx + side * (3 - 2 * mx)
         to = lax.rem(mz + dz, 4) * 16 + lax.rem(my + dy, 4) * 4 + x
         return sp_copy(pk.at[to // 2], own.at[me], a_send.at[i], own_sem.at[me], to)
@@ -237,7 +237,7 @@
         )
 
     def source(k, j, near):
-        dz, dy, side = gray(k), gray(j // 2), lax.rem(j, 2)
+        dz, dy, side = order(k), order(j // 2), lax.rem(j, 2)
         x = mx + side * (3 - 2 * mx)
         twin_x = x + 1 - 2 * lax.rem(x, 2)
         x = x if near else twin_x
@@ -292,7 +292,7 @@
         return sp_copy(pown.at[s], ret.at[slot(s)], r_send.at[s], r_recv.at[s], s)
 
     def plane(k):
-        return lax.rem(mz - gray(k) + 4, 4)
+        return lax.rem(mz - order(k) + 4, 4)
 
     def compute(k):
         z = plane(k)

time: 122 us -> 122 us (level)
  no operation moved by 1% of the time
where the time goes in v6:
time: 122 us
  Pallas kernels  121 us (99%)
    pallas_call x1, Pallas kernels, on_device(): pl.pallas_call(layer_kernel, out_shape=[jax.ShapeDtypeStruct((128, HALF),...  117 us
    pallas_call x1, Pallas kernels, on_device(): pl.pallas_call(store_kernel, out_shape=[jax.ShapeDtypeStruct(a.shape, a.d...  4.43 us

profile of v6, /device:TPU:1, one launch (start us, length us, event | category | flops | bytes accessed | tf_op | source)
XLA Modules:
  0.0 122.1 jit_solution(6195886084767543750)
XLA Ops:
  0.6 117.0 %layer.1 = (bf16[128,1024]{1,0:T(8,128)(2,1)S(1)}, f32[32,1024]{1,0:T(8,128)S(1)}, bf16[2048,896]{1,0:T(8,128)(2,1)S(1)}, bf16[2048,896]{1,0:T(8,128)(2,1)S(1)}, bf16[896,2048]{1,0:T(8,128)(2,1)S(1)}) custom-call(s32[2,128]{1,0:T(2,128)} %bitcast.13, f32[2,128]{1,0:T(2,128)} %bitcast.14, bf16[128,1024]{1,0:T(8,128)(2,1)} %stream_hbm.1, ...), custom_call_target="tpu_custom_call" | custom-call | tf_op jit(solution)/shard_map/layer/pallas_call | solution.py:613
  117.6 4.4 %store.1 = (bf16[128,1024]{1,0:T(8,128)(2,1)}, f32[32,1024]{1,0:T(8,128)}, bf16[2048,896]{1,0:T(8,128)(2,1)}, bf16[2048,896]{1,0:T(8,128)(2,1)}, bf16[896,2048]{1,0:T(8,128)(2,1)}) custom-call(bf16[128,1024]{1,0:T(8,128)(2,1)S(1)} %get-tuple-element.15.refs_0_, f32[32,1024]{1,0:T(8,128)S(1)} %get-tuple-element.16.refs_1_, ...), custom_call_target="tpu_custom_call" | custom-call | tf_op jit(solution)/shard_map/store/pallas_call | solution.py:659
